TPU v7x, 32 devices: a whole 2x2x4 slice. The times are simulated.
32 devices in a mesh: sp: 16 (over z, y, x), tp: 2 (over core).
Axes of the slice: x: 2, y: 2, z: 4, core: 2. Of those that a mesh axis runs over, the one named last changes fastest.
Arguments:
- residual: bfloat16 [4096, 2048], P(('sp', 'tp')), may hold values from -6 to 6
- query_nope: bfloat16 [4096, 1024], P('sp', 'tp'), may hold values from -24 to 24
- query_rope: bfloat16 [4096, 512], P('sp', 'tp'), may hold values from -400 to 400
- latent: bfloat16 [4096, 256], P(('sp', 'tp')), may hold values from -6 to 6
- key_rope: bfloat16 [4096, 64], P(('sp', 'tp')), may hold values from -6 to 6
- key_up: bfloat16 [256, 1024], P(None, 'tp'), may hold values from -0.375 to 0.375
- value_up: bfloat16 [256, 1024], P(None, 'tp'), may hold values from -0.375 to 0.375
- out_proj: bfloat16 [1024, 2048], replicated, may hold values from -0.375 to 0.375
- norm_gain: float32 [2048], replicated, may hold values from 0.1 to 1.9
- routes: int32 [4096, 2], P(('sp', 'tp')), may hold values from 0 to 15, all different within a row; in each aligned block of 128 rows (0 to 127, 128 to 255, ...) at most 32 rows name the same one
- route_weight: float32 [4096, 2], P(('sp', 'tp')), may hold values from 0.3 to 2.5
- w_gate: bfloat16 [16, 2048, 512], P('sp', None, 'tp'), may hold values from -0.125 to 0.125
- w_up: bfloat16 [16, 2048, 512], P('sp', None, 'tp'), may hold values from -0.125 to 0.125
- w_down: bfloat16 [16, 512, 2048], P('sp', 'tp'), may hold values from -0.25 to 0.25
Outputs:
- mixed: bfloat16 [4096, 2048], P(('sp', 'tp'))
Inputs may be any that keep to these rules, and one draw needn't show every extreme that they name: `routes`: each row names 2 different experts. Among the rows of one device no expert is named more than 32 times, a bound that some block reaches by the rows of some device.
All inputs are finite; a program needn't handle non-finite values.
Results may differ from a plain program's by a relative error of at most 0.015.
Values may be sent and summed in bfloat16 or wider, within the bound.
A program may use at most 128 MiB of HBM per device.

v0:
```python
import functools
import math

import jax
import jax.numpy as jnp
from jax import lax
from jax.experimental import pallas as pl
from jax.experimental.pallas import tpu as pltpu
from jax.sharding import PartitionSpec as P

QK_NOPE = 128
QK_ROPE = 64
V_DIM = 128
SEGMENT = 64


EPSILON = 1e-06
ROPE_BASE = 10000.0
NEG_LARGE = -1e30


def rotary(values, positions):
    half_width = values.shape[-1] // 2
    inverse = ROPE_BASE ** (-2.0 * jnp.arange(half_width, dtype=jnp.float32) / values.shape[-1])
    angles = positions.astype(jnp.float32)[:, None] * inverse[None, :]
    cosine = jnp.cos(angles)
    sine_part = jnp.sin(angles)
    if values.ndim == 3:
        cosine = cosine[:, None, :]
        sine_part = sine_part[:, None, :]
    first_half = values[..., :half_width]
    second = values[..., half_width:]
    return jnp.concatenate(
        [first_half * cosine - second * sine_part, second * cosine + first_half * sine_part],
        axis=-1,
    )


MESH = pl.DeviceIdType.MESH
VMEM = pl.BlockSpec(memory_space=pltpu.VMEM)


def greet(peers):
    barrier = pltpu.get_barrier_semaphore()
    for peer in peers:
        pl.semaphore_signal(barrier, inc=1, device_id=peer, device_id_type=MESH)
    pl.semaphore_wait(barrier, len(peers))


def far_first(count):
    return sorted(range(1, count), key=lambda step: abs(2 * step - count))


def send(source, target, send_sem, recv_sem, peer):
    copy = pltpu.make_async_remote_copy(
        src_ref=source,
        dst_ref=target,
        send_sem=send_sem,
        recv_sem=recv_sem,
        device_id=peer,
        device_id_type=MESH,
    )
    copy.start()
    return copy


def arrived(block, semaphore):
    pltpu.make_async_copy(block, block, semaphore).wait()


def gather_kernel(n_sp, n_tp, inner, own_ref, out_ref, send_sem, recv_sem, local_sem):
    sp, tp = lax.axis_index("sp"), lax.axis_index("tp")
    outer = n_sp // inner
    group, member = sp // inner, sp % inner

    def column(step):
        return ((group + step) % outer) * inner + member

    def mate(step):
        return group * inner + (member + step) % inner

    others = [(column(step), tp) for step in far_first(outer)]
    mates = [(mate(step), tp) for step in range(1, inner)]
    twins = [(sp, (tp + step) % n_tp) for step in range(1, n_tp)]
    greet(others + mates + twins)
    copies = []

    def push(source, block, peers):
        for peer in peers:
            copies.append(
                send(
                    source, out_ref.at[block], send_sem.at[len(copies)], recv_sem.at[block], peer
                )
            )

    mine = sp * n_tp + tp
    keep = pltpu.make_async_copy(own_ref, out_ref.at[mine], local_sem)
    keep.start()
    push(own_ref, mine, others + mates + twins)
    for step in sorted(range(1, outer), key=lambda step: min(step, outer - step)):
        block = column(step) * n_tp + tp
        arrived(out_ref.at[block], recv_sem.at[block])
        push(out_ref.at[block], block, mates + twins)
    for step in range(outer):
        for hop in range(1, inner):
            source = ((group + step) % outer) * inner + (member + hop) % inner
            block = source * n_tp + tp
            arrived(out_ref.at[block], recv_sem.at[block])
            push(out_ref.at[block], block, twins)
    for twin in twins:
        for source in range(n_sp):
            block = source * n_tp + twin[1]
            arrived(out_ref.at[block], recv_sem.at[block])
    keep.wait()
    for copy in copies:
        copy.wait_send()


def gather_rows(own, n_sp, n_tp):
    inner = math.gcd(n_sp, 4)
    outer = n_sp // inner
    sends = (outer - 1) + outer * (inner - 1) + n_sp * (n_tp - 1)
    return pl.pallas_call(
        functools.partial(gather_kernel, n_sp, n_tp, inner),
        out_shape=jax.ShapeDtypeStruct((n_sp * n_tp,) + own.shape, own.dtype),
        in_specs=[VMEM],
        out_specs=VMEM,
        scratch_shapes=[
            pltpu.SemaphoreType.DMA((sends,)),
            pltpu.SemaphoreType.DMA((n_sp * n_tp,)),
            pltpu.SemaphoreType.DMA,
        ],
        compiler_params=pltpu.CompilerParams(collective_id=0, has_side_effects=True),
        name="gather_rows",
    )(own)


def expert_kernel(
    n_sp,
    n_tp,
    cap,
    batch,
    rows_ref,
    gate_ref,
    up_ref,
    down_ref,
    out_ref,
    in_ref,
    part_ref,
    half_ref,
    sum_ref,
    in_send,
    in_recv,
    twin_send,
    twin_recv,
    back_send,
    back_recv,
    local_sem,
):
    sp, tp = lax.axis_index("sp"), lax.axis_index("tp")
    steps = far_first(n_sp) + [0]
    twins = [(sp, (tp + hop) % n_tp) for hop in range(1, n_tp)]
    targets = [((sp + step) % n_sp, tp) for step in steps]
    origins = [((sp + n_sp - step) % n_sp, tp) for step in steps]
    greet(targets[:-1] + twins)
    copies = []

    def span(index):
        return pl.ds(pl.multiple_of(index * cap, cap), cap)

    keep_in = pltpu.make_async_copy(
        rows_ref.at[span(sp)], in_ref.at[span((n_sp - 1) * n_tp + tp)], local_sem.at[0]
    )
    keep_in.start()
    for place in range(n_sp - 1):
        copies.append(
            send(
                rows_ref.at[span(targets[place][0])],
                in_ref.at[span(place * n_tp + tp)],
                in_send.at[place],
                in_recv.at[place * n_tp + tp],
                targets[place],
            )
        )

    def forward(place):
        block = place * n_tp + tp
        if place < n_sp - 1:
            arrived(in_ref.at[span(block)], in_recv.at[block])
        for hop, twin in enumerate(twins):
            copies.append(
                send(
                    rows_ref.at[span(sp)] if place == n_sp - 1 else in_ref.at[span(block)],
                    in_ref.at[span(block)],
                    in_send.at[n_sp - 1 + hop * n_sp + place],
                    in_recv.at[block],
                    twin,
                )
            )

    def compute(places):
        for place in places:
            for twin in twins:
                block = place * n_tp + twin[1]
                arrived(in_ref.at[span(block)], in_recv.at[block])
        if places[-1] == n_sp - 1:
            keep_in.wait()
        whole = slice(places[0] * n_tp * cap, (places[-1] + 1) * n_tp * cap)
        rows = in_ref[whole, :]
        gate = jnp.dot(rows, gate_ref[...], preferred_element_type=jnp.float32)
        up = jnp.dot(rows, up_ref[...], preferred_element_type=jnp.float32)
        activated = (gate / (1.0 + jnp.exp(-gate)) * up).astype(jnp.bfloat16)
        part_ref[whole, :] = jnp.dot(
            activated, down_ref[...], preferred_element_type=jnp.float32
        ).astype(jnp.bfloat16)
        for place in places:
            for hop, twin in enumerate(twins):
                slot = hop * n_sp + place
                copies.append(
                    send(
                        part_ref.at[span(place * n_tp + twin[1])],
                        half_ref.at[span(slot)],
                        twin_send.at[slot],
                        twin_recv.at[slot],
                        twin,
                    )
                )

    def finish(places):
        for place in places:
            value = part_ref[span(place * n_tp + tp), :].astype(jnp.float32)
            for hop in range(n_tp - 1):
                slot = hop * n_sp + place
                arrived(half_ref.at[span(slot)], twin_recv.at[slot])
                value = value + half_ref[span(slot), :].astype(jnp.float32)
            if place == n_sp - 1:
                out_ref[span(sp), :] = value.astype(out_ref.dtype)
            else:
                sum_ref[span(place), :] = value.astype(sum_ref.dtype)
                copies.append(
                    send(
                        sum_ref.at[span(place)],
                        out_ref.at[span(sp)],
                        back_send.at[place],
                        back_recv.at[sp],
                        origins[place],
                    )
                )

    batches = [list(range(n_sp))[first : first + batch] for first in range(0, n_sp, batch)]
    for place in batches[0]:
        forward(place)
    for number, places in enumerate(batches):
        compute(places)
        if number > 0:
            finish(batches[number - 1])
        if number + 1 < len(batches):
            for place in batches[number + 1]:
                forward(place)
    finish(batches[-1])
    for target in targets[:-1]:
        arrived(out_ref.at[span(target[0])], back_recv.at[target[0]])
    for copy in copies:
        copy.wait_send()


def expert_rows(rows, gate, up, down, n_sp, n_tp):
    cap = rows.shape[0] // n_sp
    width = rows.shape[1]
    dma = pltpu.SemaphoreType.DMA
    return pl.pallas_call(
        functools.partial(expert_kernel, n_sp, n_tp, cap, math.gcd(n_sp, 256 // (n_tp * cap))),
        out_shape=jax.ShapeDtypeStruct(rows.shape, rows.dtype),
        in_specs=[VMEM] * 4,
        out_specs=VMEM,
        scratch_shapes=[
            pltpu.VMEM((n_sp * n_tp * cap, width), rows.dtype),
            pltpu.VMEM((n_sp * n_tp * cap, width), rows.dtype),
            pltpu.VMEM((n_sp * (n_tp - 1) * cap, width), rows.dtype),
            pltpu.VMEM(rows.shape, rows.dtype),
            dma((n_sp - 1 + n_sp * (n_tp - 1),)),
            dma((n_sp * n_tp,)),
            dma((n_sp * (n_tp - 1),)),
            dma((n_sp * (n_tp - 1),)),
            dma((n_sp - 1,)),
            dma((n_sp,)),
            dma((1,)),
        ],
        compiler_params=pltpu.CompilerParams(collective_id=1, has_side_effects=True),
        name="expert_rows",
    )(rows, gate, up, down)


def heads_kernel(n_tp, own_ref, out_ref, send_sem, recv_sem, local_sem):
    sp, tp = lax.axis_index("sp"), lax.axis_index("tp")
    twins = [(sp, (tp + hop) % n_tp) for hop in range(1, n_tp)]
    greet(twins)
    rows = out_ref.shape[1]

    def part(core):
        return own_ref.at[pl.ds(pl.multiple_of(core * rows, rows), rows)]

    copies = [
        send(part(twin[1]), out_ref.at[tp], send_sem.at[hop], recv_sem.at[tp], twin)
        for hop, twin in enumerate(twins)
    ]
    keep = pltpu.make_async_copy(part(tp), out_ref.at[tp], local_sem)
    keep.start()
    for twin in twins:
        arrived(out_ref.at[twin[1]], recv_sem.at[twin[1]])
    keep.wait()
    for copy in copies:
        copy.wait_send()


def swap_heads(own, n_tp):
    return pl.pallas_call(
        functools.partial(heads_kernel, n_tp),
        out_shape=jax.ShapeDtypeStruct((n_tp, own.shape[0] // n_tp, own.shape[1]), own.dtype),
        in_specs=[VMEM],
        out_specs=VMEM,
        scratch_shapes=[
            pltpu.SemaphoreType.DMA((n_tp - 1,)),
            pltpu.SemaphoreType.DMA((n_tp,)),
            pltpu.SemaphoreType.DMA,
        ],
        compiler_params=pltpu.CompilerParams(collective_id=2, has_side_effects=True),
        name="swap_heads",
    )(own)


NT = (((1,), (1,)), ((), ()))


def attention_kernel(
    key_block, latent_width, heads, base_ref, query_ref, kv_ref, key_up_ref, value_up_ref, out_ref, max_ref, sum_ref, acc_ref
):
    first = base_ref[0]
    queries = query_ref.shape[2]
    scale = (QK_NOPE + QK_ROPE) ** (-0.5) * math.log2(math.e)
    max_ref[...] = jnp.full_like(max_ref, NEG_LARGE)
    sum_ref[...] = jnp.zeros_like(sum_ref)
    acc_ref[...] = jnp.zeros_like(acc_ref)

    def block(start, masked):
        start = pl.multiple_of(start, key_block)
        rows = kv_ref[pl.ds(start, key_block), :]
        latent = rows[:, :latent_width]
        rot = rows[:, latent_width:]
        keys = jnp.dot(latent, key_up_ref[...], preferred_element_type=jnp.float32).astype(
            jnp.bfloat16
        )
        values = lax.dot_general(
            value_up_ref[...], latent, NT, preferred_element_type=jnp.float32
        ).astype(jnp.bfloat16)
        if masked:
            key_segment = (
                start + lax.broadcasted_iota(jnp.int32, (key_block, queries), 0)
            ) // SEGMENT
            query_segment = (
                first + lax.broadcasted_iota(jnp.int32, (key_block, queries), 1)
            ) // SEGMENT
            allowed = key_segment <= query_segment
        for head in range(heads):
            wide = jnp.concatenate([keys[:, head * QK_NOPE : (head + 1) * QK_NOPE], rot], axis=1)
            scores = jnp.dot(wide, query_ref[head], preferred_element_type=jnp.float32)
            if masked:
                scores = jnp.where(allowed, scores, NEG_LARGE)
            old_max = max_ref[head]
            new_max = jnp.maximum(old_max, jnp.max(scores, axis=0, keepdims=True))
            weights = jnp.exp2((scores - new_max) * scale)
            shrink = jnp.exp2((old_max - new_max) * scale)
            max_ref[head] = new_max
            sum_ref[head] = sum_ref[head] * shrink + jnp.sum(weights, axis=0, keepdims=True)
            acc_ref[head] = acc_ref[head] * shrink + jnp.dot(
                values[head * V_DIM : (head + 1) * V_DIM],
                weights.astype(jnp.bfloat16),
                preferred_element_type=jnp.float32,
            )

    whole = first // key_block

    def body(step, carry):
        block(step * key_block, False)
        return carry

    lax.fori_loop(0, whole, body, 0)
    block(whole * key_block, True)
    for head in range(heads):
        out_ref[:, head * V_DIM : (head + 1) * V_DIM] = (
            (acc_ref[head] / sum_ref[head]).T.astype(out_ref.dtype)
        )


def attention(base, query, kv, key_up, value_up_t, key_block, latent_width):
    heads, unused, queries = query.shape
    return pl.pallas_call(
        functools.partial(attention_kernel, key_block, latent_width, heads),
        out_shape=jax.ShapeDtypeStruct((queries, heads * V_DIM), jnp.bfloat16),
        in_specs=[pl.BlockSpec(memory_space=pltpu.SMEM), VMEM, VMEM, VMEM, VMEM],
        out_specs=VMEM,
        scratch_shapes=[
            pltpu.VMEM((heads, 1, queries), jnp.float32),
            pltpu.VMEM((heads, 1, queries), jnp.float32),
            pltpu.VMEM((heads, V_DIM, queries), jnp.float32),
        ],
        name="attention",
    )(base, query, kv, key_up, value_up_t)


def local(
    residual,
    query_nope,
    query_rope,
    latent,
    key_rope,
    key_up,
    value_up,
    out_proj,
    norm_gain,
    routes,
    route_weight,
    w_gate,
    w_up,
    w_down,
):
    tp_count = lax.axis_size("tp")
    sp_count = lax.axis_size("sp")
    tp_index = lax.axis_index("tp")
    sp_index = lax.axis_index("sp")
    row_count = residual.shape[0]
    tok_dev = query_nope.shape[0]
    heads_here = query_nope.shape[1] // QK_NOPE
    query_first = sp_index * tok_dev
    query_pos = query_first + jnp.arange(tok_dev, dtype=jnp.int32)
    query_rot = rotary(
        query_rope.astype(jnp.float32).reshape(tok_dev, heads_here, QK_ROPE), query_pos
    ).astype(jnp.bfloat16)
    query_heads = query_nope.reshape(tok_dev, heads_here, QK_NOPE)
    key_pos = query_first + tp_index * row_count + jnp.arange(row_count, dtype=jnp.int32)
    key_rot = rotary(key_rope.astype(jnp.float32), key_pos).astype(jnp.bfloat16)
    width_pad = -(-QK_ROPE // 128) * 128 - QK_ROPE
    packed = jnp.concatenate(
        [latent, key_rot, jnp.zeros((row_count, width_pad), jnp.bfloat16)], axis=1
    )
    gathered = gather_rows(packed, sp_count, tp_count)
    kv_rows = gathered.reshape(sp_count * tok_dev, packed.shape[1])
    query = jnp.concatenate(
        [query_heads, query_rot, jnp.zeros((tok_dev, heads_here, width_pad), jnp.bfloat16)], axis=2
    ).transpose(1, 2, 0)
    key_block = tok_dev * math.gcd(sp_count, 2)
    attn_out = attention(
        query_first.astype(jnp.int32).reshape(1),
        query,
        kv_rows,
        key_up,
        value_up.T,
        key_block,
        latent.shape[1],
    )
    all_heads = swap_heads(attn_out, tp_count)
    proj_parts = out_proj.reshape(tp_count, attn_out.shape[1], out_proj.shape[1])
    projected = jnp.dot(all_heads[0], proj_parts[0], preferred_element_type=jnp.float32)
    for core in range(1, tp_count):
        projected = projected + jnp.dot(
            all_heads[core], proj_parts[core], preferred_element_type=jnp.float32
        )
    hidden_wide = residual.astype(jnp.float32) + projected
    hidden = hidden_wide.astype(jnp.bfloat16)
    hidden_wide = hidden.astype(jnp.float32)
    normed = hidden_wide * lax.rsqrt(
        jnp.mean(hidden_wide * hidden_wide, axis=-1, keepdims=True) + EPSILON
    )
    normed = (normed * norm_gain[None, :]).astype(jnp.bfloat16)
    expert_count = lax.axis_size("sp")
    capacity = max(2, 2 * (row_count * tp_count) // expert_count)
    capacity = -(-capacity // 16) * 16
    top_count = routes.shape[1]
    width = normed.shape[1]
    flat_expert = routes.reshape(-1)
    onehot = (flat_expert[:, None] == jnp.arange(expert_count, dtype=jnp.int32)[None, :]).astype(
        jnp.int32
    )
    slot_rank = jnp.sum(jnp.cumsum(onehot, axis=0) * onehot, axis=1) - 1
    slot_index = flat_expert * capacity + slot_rank
    slots = slot_index.reshape(row_count, top_count)
    slot_count = expert_count * capacity
    numbers = jnp.arange(slot_count, dtype=jnp.int32)
    chosen = slots[:, :, None] == numbers[None, None, :]
    place = jnp.any(chosen, axis=1).astype(jnp.bfloat16)
    outgoing = lax.dot_general(
        place, normed, (((0,), (0,)), ((), ())), preferred_element_type=jnp.float32
    ).astype(jnp.bfloat16)
    shares = jnp.sum(jnp.where(chosen, route_weight[:, :, None], 0.0), axis=1)
    share_high = lax.reduce_precision(shares, 8, 7)
    share_low = shares - share_high
    back_rows = expert_rows(outgoing, w_gate[0], w_up[0], w_down[0], sp_count, tp_count)
    combined = jnp.dot(
        share_high.astype(jnp.bfloat16), back_rows, preferred_element_type=jnp.float32
    ) + jnp.dot(share_low.astype(jnp.bfloat16), back_rows, preferred_element_type=jnp.float32)
    return (hidden_wide + combined).astype(jnp.bfloat16)


def solution(mesh):
    return jax.shard_map(
        local,
        mesh=mesh,
        in_specs=(
            P(("sp", "tp"), None),
            P("sp", "tp"),
            P("sp", "tp"),
            P(("sp", "tp"), None),
            P(("sp", "tp"), None),
            P(None, "tp"),
            P(None, "tp"),
            P(),
            P(),
            P(("sp", "tp"), None),
            P(("sp", "tp"), None),
            P("sp", None, "tp"),
            P("sp", None, "tp"),
            P("sp", "tp", None),
        ),
        out_specs=P(("sp", "tp"), None),
        check_vma=False,
    )
```

profile of v0, /device:TPU:16, one launch (start us, length us, event | category | flops | bytes accessed | tf_op | source)
XLA Modules:
  0.0 175.2 jit_solution(7350379490422024057)
XLA Ops:
  0.0 0.0 copy-start.5
  0.0 0.0 copy-start.4
  0.0 0.2 multiply_cosine_fusion.1
  0.2 1.0 copy.42
  1.3 0.1 pad.7.clone
  1.4 1.1 copy.41
  2.5 0.9 maximum_bitcast_fusion.query_ref
  3.4 0.0 copy-start.3
  3.4 0.0 copy-done.5
  3.4 0.1 copy.43
  3.5 0.3 fusion.23
  3.9 0.1 pad.3.clone
  3.9 0.0 copy-done.4
  3.9 0.7 maximum_maximum_fusion.own_ref
  4.7 28.6 %gather_rows.1 = bf16[32,128,384]{2,1,0:T(8,128)(2,1)} custom-call(bf16[128,384]{1,0:T(8,128)(2,1)} %maximum_maximum_fusion.own_ref), custom_call_target="tpu_custom_call" | custom-call | tf_op jit(solution)/shard_map/gather_rows/pallas_call | solution.py:123
  33.2 0.0 copy-done.3
  33.2 0.8 copy.45
  34.1 13.4 %attention.1.own_ref = bf16[256,512]{1,0:T(8,128)(2,1)} custom-call(s32[1]{0:T(128)} %bitcast.base_ref, bf16[4,256,256]{2,1,0:T(8,128)(2,1)} %maximum_bitcast_fusion.query_ref, bf16[4096,384]{1,0:T(8,128)(2,1)} %bitcast.36, bf16[256,512]{1,0:T(8,128)(2,1)} %key_up_ref.1, bf16[512,256]{1,0:T(8,128)(2,1)} %bitcast.42), custom_call_target="tpu_custom_call" | custom-call | tf_op jit(solution)/shard_map/attention/pallas_call | solution.py:397
  47.5 0.0 copy-start.2
  47.5 3.2 %swap_heads.1 = bf16[2,128,512]{2,1,0:T(8,128)(2,1)} custom-call(bf16[256,512]{1,0:T(8,128)(2,1)} %attention.1.own_ref), custom_call_target="tpu_custom_call" | custom-call | tf_op jit(solution)/shard_map/swap_heads/pallas_call | solution.py:317
  50.7 0.0 copy-start.1
  50.7 2.2 %fusion.6 = f32[128,2048]{1,0:T(8,128)S(1)} fusion(bf16[1024,2048]{1,0:T(8,128)(2,1)} %param.21, bf16[2,128,512]{2,1,0:T(8,128)(2,1)} %swap_heads.1), kind=kOutput, calls=%fused_computation.9 | convolution fusion | flops 268435456 | bytes 3276800 | tf_op jit(solution)/shard_map/dot_general | solution.py:463
  52.8 0.0 copy-done.2
  52.8 0.0 copy-done.1
  52.9 0.0 copy-start.7
  52.9 0.0 copy-start.6
  52.9 2.3 %multiply_reduce_fusion = (f32[128]{0:T(128)S(1)}, f32[128,2048]{1,0:T(8,128)S(1)}) fusion(f32[128,2048]{1,0:T(8,128)S(1)} %fusion.6, bf16[1024,2048]{1,0:T(8,128)(2,1)} %param.21, bf16[2,128,512]{2,1,0:T(8,128)(2,1)S(1)} %copy-done.1, bf16[128,2048]{1,0:T(8,128)(2,1)S(1)} %copy-done.2), kind=kOutput, calls=%fused_computation.12 | convolution fusion | flops 270270336 | bytes 4850176 | tf_op jit(solution)/shard_map/dot_general | solution.py:465
  55.2 0.0 copy-done.7
  55.2 0.1 copy.46
  55.3 0.1 eq.42
  55.4 0.6 reduce-window.6
  56.0 0.2 slice_reduce_fusion
  56.3 0.1 eq.38
  56.4 0.1 fusion.27
  56.5 0.1 sub.18
  56.6 0.1 copy.49
  56.7 0.1 fusion.10
  56.9 0.0 copy-done.6
  56.9 2.1 %convolution_convert_fusion.rows_ref = bf16[512,2048]{1,0:T(8,128)(2,1)} fusion(pred[128,512]{1,0:T(8,128)(4,1)S(1)} %fusion.10, f32[128,2048]{1,0:T(8,128)S(1)} %get-tuple-element.12, f32[2048]{0:T(1024)S(1)} %copy-done.6, f32[128]{0:T(128)S(1)} %add_rsqrt_fusion), kind=kOutput, calls=%fused_computation | convolution fusion | flops 270270464 | bytes 3219968 | tf_op jit(solution)/shard_map/dot_general | solution.py:491
  59.0 0.0 copy-start.8
  59.0 112.6 %expert_rows.1 = bf16[512,2048]{1,0:T(8,128)(2,1)} custom-call(bf16[512,2048]{1,0:T(8,128)(2,1)} %convolution_convert_fusion.rows_ref, bf16[2048,256]{1,0:T(8,128)(2,1)} %bitcast.37, bf16[2048,256]{1,0:T(8,128)(2,1)} %bitcast.38, bf16[256,2048]{1,0:T(8,128)(2,1)} %bitcast.39), custom_call_target="tpu_custom_call" | custom-call | tf_op jit(solution)/shard_map/expert_rows/pallas_call | solution.py:271
  171.6 0.0 copy-done.8
  171.6 0.0 copy-start
  171.6 0.1 select_reduce_fusion
  171.8 2.2 %fusion.13 = f32[128,2048]{1,0:T(8,128)S(1)} fusion(bf16[512,2048]{1,0:T(8,128)(2,1)} %expert_rows.1, f32[128,512]{1,0:T(8,128)S(1)} %select_reduce_fusion), kind=kOutput, calls=%fused_computation.22 | convolution fusion | flops 268566528 | bytes 3407872 | tf_op jit(solution)/shard_map/dot_general | solution.py:498
  173.9 0.0 copy-done
  173.9 1.3 fusion.4
  (12 shorter events, 0.1 us)
Async XLA Ops:
  0.0 3.4 %copy-start.5 = (bf16[128,64]{0,1:T(8,128)(2,1)S(1)}, bf16[128,64]{0,1:T(8,128)(2,1)}, u32[]{:S(2)}) copy-start(bf16[128,64]{0,1:T(8,128)(2,1)} %param.18) | copy-start | bytes 49156
  0.0 3.9 %copy-start.4 = (bf16[128,256]{1,0:T(8,128)(2,1)S(1)}, bf16[128,256]{1,0:T(8,128)(2,1)}, u32[]{:S(2)}) copy-start(bf16[128,256]{1,0:T(8,128)(2,1)} %param.17) | copy-start | bytes 196612
  3.4 29.8 %copy-start.3 = (bf16[256,512]{1,0:T(8,128)(2,1)S(1)}, bf16[256,512]{1,0:T(8,128)(2,1)}, u32[]{:S(2)}) copy-start(bf16[256,512]{1,0:T(8,128)(2,1)} %param.20) | copy-start | bytes 786436
  47.5 5.3 %copy-start.2 = (bf16[128,2048]{1,0:T(8,128)(2,1)S(1)}, bf16[128,2048]{1,0:T(8,128)(2,1)}, u32[]{:S(2)}) copy-start(bf16[128,2048]{1,0:T(8,128)(2,1)} %param.14) | copy-start | bytes 1572868
  50.7 2.2 %copy-start.1 = (bf16[2,128,512]{2,1,0:T(8,128)(2,1)S(1)}, bf16[2,128,512]{2,1,0:T(8,128)(2,1)}, u32[]{:S(2)}) copy-start(bf16[2,128,512]{2,1,0:T(8,128)(2,1)} %swap_heads.1) | copy-start | bytes 786436
  52.9 2.3 %copy-start.7 = (s32[128,2]{0,1:T(2,128)S(1)}, s32[128,2]{0,1:T(2,128)}, u32[]{:S(2)}) copy-start(s32[128,2]{0,1:T(2,128)} %param.23) | copy-start | bytes 3076
  52.9 4.0 %copy-start.6 = (f32[2048]{0:T(1024)S(1)}, f32[2048]{0:T(1024)}, u32[]{:S(2)}) copy-start(f32[2048]{0:T(1024)} %param.22) | copy-start | bytes 24580
  59.0 112.6 %copy-start.8 = (f32[128,2]{0,1:T(2,128)S(1)}, f32[128,2]{0,1:T(2,128)}, u32[]{:S(2)}) copy-start(f32[128,2]{0,1:T(2,128)} %param.24) | copy-start | bytes 3076
  171.6 2.3 %copy-start = (bf16[512,2048]{1,0:T(8,128)(2,1)S(1)}, bf16[512,2048]{1,0:T(8,128)(2,1)}, u32[]{:S(2)}) copy-start(bf16[512,2048]{1,0:T(8,128)(2,1)} %expert_rows.1) | copy-start | bytes 6291460
where the time goes:
time: 176 us; the launch traced here: 175 us
  Pallas kernels  158 us (90%)
  matrix products  10 us (6%)
  local copies, waits for them, and re-layouts  4.03 us (2%)
  other arithmetic  3.26 us (2%)
    pallas_call x1, Pallas kernels, expert_rows(): pl.pallas_call(functools.partial(expert_kernel, n_sp, n_tp, cap, math.gcd...  113 us
    pallas_call x1, Pallas kernels, gather_rows(): pl.pallas_call(functools.partial(gather_kernel, n_sp, n_tp, inner), out_s...  28.6 us
    pallas_call x1, Pallas kernels, attention(): pl.pallas_call(functools.partial(attention_kernel, key_block, latent_widt...  13.4 us

commit v1 on v0

--- a/solution.py
+++ b/solution.py
@@ -135,160 +135,383 @@
     )(own)
 
 
-def expert_kernel(
-    n_sp,
+def moe_kernel(
+    n_outer,
+    n_inner,
     n_tp,
-    cap,
-    batch,
-    rows_ref,
+    chunks,
+    tok_ref,
+    meta_ref,
+    hidden_ref,
     gate_ref,
     up_ref,
     down_ref,
     out_ref,
+    tok_all,
+    meta_all,
+    disp_ref,
     in_ref,
+    made_ref,
+    back_ref,
     part_ref,
-    half_ref,
-    sum_ref,
-    in_send,
-    in_recv,
-    twin_send,
-    twin_recv,
+    sum_in,
+    gate_all,
+    up_all,
+    down_all,
+    meta_send,
+    meta_recv,
+    above_send,
+    below_send,
+    tok_recv,
+    disp_send,
+    disp_recv,
     back_send,
     back_recv,
-    local_sem,
+    sum_send,
+    sum_recv,
+    weight_send,
+    weight_recv,
 ):
     sp, tp = lax.axis_index("sp"), lax.axis_index("tp")
-    steps = far_first(n_sp) + [0]
+    group, member = sp // n_inner, sp % n_inner
+    rows = tok_ref.shape[0]
+    width = tok_ref.shape[1] // chunks
+    slots = disp_ref.shape[2]
+    cap = slots // n_inner
+    last = n_outer - 1
+    has_above, has_below = group < last, group > 0
+
+    def at(plane, place):
+        return (plane * n_inner + place, tp)
+
+    others = [at((group + step) % n_outer, member) for step in range(1, n_outer)]
+    mates = [(member + step) % n_inner for step in range(1, n_inner)]
     twins = [(sp, (tp + hop) % n_tp) for hop in range(1, n_tp)]
-    targets = [((sp + step) % n_sp, tp) for step in steps]
-    origins = [((sp + n_sp - step) % n_sp, tp) for step in steps]
-    greet(targets[:-1] + twins)
-    copies = []
-
-    def span(index):
-        return pl.ds(pl.multiple_of(index * cap, cap), cap)
-
-    keep_in = pltpu.make_async_copy(
-        rows_ref.at[span(sp)], in_ref.at[span((n_sp - 1) * n_tp + tp)], local_sem.at[0]
-    )
-    keep_in.start()
-    for place in range(n_sp - 1):
-        copies.append(
-            send(
-                rows_ref.at[span(targets[place][0])],
-                in_ref.at[span(place * n_tp + tp)],
-                in_send.at[place],
-                in_recv.at[place * n_tp + tp],
-                targets[place],
+    greet(others + [at(group, mate) for mate in mates] + twins)
+
+    def copy(source, target, send_sem, recv_sem, peer):
+        return pltpu.make_async_remote_copy(
+            src_ref=source,
+            dst_ref=target,
+            send_sem=send_sem,
+            recv_sem=recv_sem,
+            device_id=peer,
+            device_id_type=MESH,
+        )
+
+    def span(place):
+        return pl.ds(pl.multiple_of(place * cap, cap), cap)
+
+    def meta_copy(step):
+        return copy(
+            meta_ref, meta_all.at[group], meta_send.at[step], meta_recv.at[group], others[step]
+        )
+
+    def relay(block, chunk, upward):
+        sems = above_send if upward else below_send
+        ref = tok_all.at[block, chunk]
+        number = block * chunks + chunk
+        peer = at(group + 1 if upward else group - 1, member)
+        return copy(ref, ref, sems.at[number], tok_recv.at[number], peer)
+
+    def plane_copy(source, target, send_sem, recv_sem, block, chunk, mate):
+        number = (block * chunks + chunk) * n_inner
+        return copy(
+            source.at[block, chunk, span(mate)],
+            target.at[block, chunk, span(member)],
+            send_sem.at[number + mate],
+            recv_sem.at[number + member],
+            at(group, mate),
+        )
+
+    def disp_copy(block, chunk, mate):
+        return plane_copy(disp_ref, in_ref, disp_send, disp_recv, block, chunk, mate)
+
+    def back_copy(block, chunk, mate):
+        return plane_copy(made_ref, back_ref, back_send, back_recv, block, chunk, mate)
+
+    def plane_arrived(target, recv_sem, block, chunk):
+        for mate in mates:
+            arrived(
+                target.at[block, chunk, span(mate)],
+                recv_sem.at[(block * chunks + chunk) * n_inner + mate],
             )
-        )
-
-    def forward(place):
-        block = place * n_tp + tp
-        if place < n_sp - 1:
-            arrived(in_ref.at[span(block)], in_recv.at[block])
+
+    def sum_copy(block, chunk, downward):
+        slot = jnp.where(downward | (block != group + 1), block, n_outer)
+        peer = at(jnp.where(downward, group - 1, group + 1), member)
+        return copy(
+            part_ref.at[block, chunk],
+            sum_in.at[slot, chunk],
+            sum_send.at[block * chunks + chunk],
+            sum_recv.at[slot * chunks + chunk],
+            peer,
+        )
+
+    weights = [(gate_ref, gate_all), (up_ref, up_all), (down_ref, down_all)]
+
+    def weight_copies():
         for hop, twin in enumerate(twins):
-            copies.append(
-                send(
-                    rows_ref.at[span(sp)] if place == n_sp - 1 else in_ref.at[span(block)],
-                    in_ref.at[span(block)],
-                    in_send.at[n_sp - 1 + hop * n_sp + place],
-                    in_recv.at[block],
-                    twin,
+            for number, (own, everyone) in enumerate(weights):
+                slot = hop * 3 + number
+                yield copy(
+                    own, everyone.at[hop], weight_send.at[slot], weight_recv.at[slot], twin
                 )
+
+    first_slot = (group * slots).astype(jnp.float32)
+
+    def named(block):
+        numbers = first_slot + lax.broadcasted_iota(jnp.int32, (slots, rows), 0).astype(
+            jnp.float32
+        )
+        meta = meta_all[block]
+        return meta[0:1] == numbers, meta[1:2] == numbers, meta
+
+    def scatter(block, chunk):
+        one, two, unused = named(block)
+        place = jnp.where(one | two, 1.0, 0.0).astype(jnp.bfloat16)
+        disp_ref[block, chunk] = jnp.dot(
+            place, tok_all[block, chunk], preferred_element_type=jnp.float32
+        ).astype(jnp.bfloat16)
+        for mate in mates:
+            disp_copy(block, chunk, mate).start()
+        in_ref[block, chunk, span(member)] = disp_ref[block, chunk, span(member)]
+
+    def expert(block):
+        for chunk in range(chunks):
+            plane_arrived(in_ref, disp_recv, block, chunk)
+        inputs = jnp.concatenate([in_ref[block, chunk] for chunk in range(chunks)], axis=1)
+        halves = []
+        for hop in range(n_tp):
+            gate_half = gate_ref[...] if hop == 0 else gate_all[hop - 1]
+            up_half = up_ref[...] if hop == 0 else up_all[hop - 1]
+            gate = jnp.dot(inputs, gate_half, preferred_element_type=jnp.float32)
+            up = jnp.dot(inputs, up_half, preferred_element_type=jnp.float32)
+            halves.append((gate / (1.0 + jnp.exp(-gate)) * up).astype(jnp.bfloat16))
+        for chunk in range(chunks):
+            columns = slice(chunk * width, (chunk + 1) * width)
+            made = jnp.dot(halves[0], down_ref[:, columns], preferred_element_type=jnp.float32)
+            for hop in range(1, n_tp):
+                made = made + jnp.dot(
+                    halves[hop], down_all[hop - 1, :, columns], preferred_element_type=jnp.float32
+                )
+            made_ref[block, chunk] = made.astype(jnp.bfloat16)
+            for mate in mates:
+                back_copy(block, chunk, mate).start()
+            back_ref[block, chunk, span(member)] = made_ref[block, chunk, span(member)]
+
+    def weighted(block, chunk):
+        one, two, meta = named(block)
+        shares = jnp.where(one, meta[2:3], 0.0) + jnp.where(two, meta[3:4], 0.0)
+        high = shares.astype(jnp.bfloat16)
+        low = (shares - high.astype(jnp.float32)).astype(jnp.bfloat16)
+        plane_arrived(back_ref, back_recv, block, chunk)
+        values = back_ref[block, chunk]
+        return lax.dot_general(high, values, TN, preferred_element_type=jnp.float32) + (
+            lax.dot_general(low, values, TN, preferred_element_type=jnp.float32)
+        )
+
+    def start_sum(block):
+        downward = block < group
+
+        @pl.when((downward & (group == last)) | ((block > group) & (group == 0)))
+        def _():
+            for chunk in range(chunks):
+                part_ref[block, chunk] = weighted(block, chunk).astype(jnp.bfloat16)
+                sum_copy(block, chunk, downward).start()
+
+    def pass_sum(valid, block, chunk, downward):
+        @pl.when(valid)
+        def _():
+            total = weighted(block, chunk)
+            arrived(sum_in.at[block, chunk], sum_recv.at[block * chunks + chunk])
+            part_ref[block, chunk] = (
+                total + sum_in[block, chunk].astype(jnp.float32)
+            ).astype(jnp.bfloat16)
+            sum_copy(block, chunk, downward).start()
+
+    def both(distance, action):
+        @pl.when(group >= distance)
+        def _():
+            action(group - distance)
+
+        @pl.when((distance > 0) & (group + distance < n_outer))
+        def _():
+            action(group + distance)
+
+    meta_all[group] = meta_ref[...]
+    for step in range(n_outer - 1):
+        meta_copy(step).start()
+    for chunk in range(chunks):
+        tok_all[group, chunk] = tok_ref[:, chunk * width : (chunk + 1) * width]
+
+        @pl.when(has_above)
+        def _():
+            relay(group, chunk, True).start()
+
+        @pl.when(has_below)
+        def _():
+            relay(group, chunk, False).start()
+
+    for item in weight_copies():
+        item.start()
+    for chunk in range(chunks):
+        scatter(group, chunk)
+
+    def receive(block, chunk, upward):
+        number = block * chunks + chunk
+        arrived(tok_all.at[block, chunk], tok_recv.at[number])
+        if chunk == 0:
+            arrived(meta_all.at[block], meta_recv.at[block])
+
+        @pl.when(has_above if upward else has_below)
+        def _():
+            relay(block, chunk, upward).start()
+
+        scatter(block, chunk)
+
+    def stage(distance, carry):
+        for chunk in range(chunks):
+
+            @pl.when(group >= distance)
+            def _():
+                receive(group - distance, chunk, True)
+
+            @pl.when(group + distance < n_outer)
+            def _():
+                receive(group + distance, chunk, False)
+
+            if chunk == EXPERT_LAG % chunks:
+
+                @pl.when(distance == 1)
+                def _():
+                    for item in weight_copies():
+                        item.wait_recv()
+
+                both(distance - 1, expert)
+            if chunk == SUM_LAG % chunks:
+                both(distance - 1, start_sum)
+        return carry
+
+    lax.fori_loop(1, n_outer, stage, 0)
+    both(last, expert)
+    both(last, start_sum)
+
+    def sum_stage(distance, carry):
+        low_first = 2 * group >= n_outer
+        low, high = last - distance, distance + 0
+        low_valid = (low < group) & has_above
+        high_valid = (high > group) & has_below
+        first = jnp.where(low_first, low, high)
+        second = jnp.where(low_first, high, low)
+        first_valid = (low_first & low_valid) | (jnp.logical_not(low_first) & high_valid)
+        second_valid = (low_first & high_valid) | (jnp.logical_not(low_first) & low_valid)
+        lag = chunks // 2
+        for step in range(chunks + lag):
+            if step < chunks:
+                pass_sum(first_valid, first, step, first < group)
+            if step >= lag:
+                pass_sum(second_valid, second, step - lag, second < group)
+        return carry
+
+    lax.fori_loop(1, n_outer, sum_stage, 0)
+
+    for chunk in range(chunks):
+        columns = slice(chunk * width, (chunk + 1) * width)
+        total = weighted(group, chunk) + hidden_ref[:, columns].astype(jnp.float32)
+        sides = []
+        for side, slot in ((has_above, group), (has_below, n_outer)):
+
+            @pl.when(side)
+            def _(slot=slot):
+                arrived(sum_in.at[slot, chunk], sum_recv.at[slot * chunks + chunk])
+
+            sides.append(
+                jnp.where(side, sum_in[slot, chunk].astype(jnp.float32), 0.0)
             )
-
-    def compute(places):
-        for place in places:
-            for twin in twins:
-                block = place * n_tp + twin[1]
-                arrived(in_ref.at[span(block)], in_recv.at[block])
-        if places[-1] == n_sp - 1:
-            keep_in.wait()
-        whole = slice(places[0] * n_tp * cap, (places[-1] + 1) * n_tp * cap)
-        rows = in_ref[whole, :]
-        gate = jnp.dot(rows, gate_ref[...], preferred_element_type=jnp.float32)
-        up = jnp.dot(rows, up_ref[...], preferred_element_type=jnp.float32)
-        activated = (gate / (1.0 + jnp.exp(-gate)) * up).astype(jnp.bfloat16)
-        part_ref[whole, :] = jnp.dot(
-            activated, down_ref[...], preferred_element_type=jnp.float32
-        ).astype(jnp.bfloat16)
-        for place in places:
-            for hop, twin in enumerate(twins):
-                slot = hop * n_sp + place
-                copies.append(
-                    send(
-                        part_ref.at[span(place * n_tp + twin[1])],
-                        half_ref.at[span(slot)],
-                        twin_send.at[slot],
-                        twin_recv.at[slot],
-                        twin,
-                    )
-                )
-
-    def finish(places):
-        for place in places:
-            value = part_ref[span(place * n_tp + tp), :].astype(jnp.float32)
-            for hop in range(n_tp - 1):
-                slot = hop * n_sp + place
-                arrived(half_ref.at[span(slot)], twin_recv.at[slot])
-                value = value + half_ref[span(slot), :].astype(jnp.float32)
-            if place == n_sp - 1:
-                out_ref[span(sp), :] = value.astype(out_ref.dtype)
-            else:
-                sum_ref[span(place), :] = value.astype(sum_ref.dtype)
-                copies.append(
-                    send(
-                        sum_ref.at[span(place)],
-                        out_ref.at[span(sp)],
-                        back_send.at[place],
-                        back_recv.at[sp],
-                        origins[place],
-                    )
-                )
-
-    batches = [list(range(n_sp))[first : first + batch] for first in range(0, n_sp, batch)]
-    for place in batches[0]:
-        forward(place)
-    for number, places in enumerate(batches):
-        compute(places)
-        if number > 0:
-            finish(batches[number - 1])
-        if number + 1 < len(batches):
-            for place in batches[number + 1]:
-                forward(place)
-    finish(batches[-1])
-    for target in targets[:-1]:
-        arrived(out_ref.at[span(target[0])], back_recv.at[target[0]])
-    for copy in copies:
-        copy.wait_send()
-
-
-def expert_rows(rows, gate, up, down, n_sp, n_tp):
-    cap = rows.shape[0] // n_sp
-    width = rows.shape[1]
+        out_ref[:, columns] = (total + sides[0] + sides[1]).astype(out_ref.dtype)
+
+    for step in range(n_outer - 1):
+        meta_copy(step).wait_send()
+    for item in weight_copies():
+        item.wait_send()
+
+    def drain(block, carry):
+        for chunk in range(chunks):
+
+            @pl.when(has_above & (block <= group))
+            def _():
+                relay(block, chunk, True).wait_send()
+
+            @pl.when(has_below & (block >= group))
+            def _():
+                relay(block, chunk, False).wait_send()
+
+            for mate in mates:
+                disp_copy(block, chunk, mate).wait_send()
+                back_copy(block, chunk, mate).wait_send()
+
+            @pl.when(block != group)
+            def _():
+                sum_copy(block, chunk, block < group).wait_send()
+
+        return carry
+
+    lax.fori_loop(0, n_outer, drain, 0)
+
+
+EXPERT_LAG = 0
+SUM_LAG = 1
+TN = (((0,), (0,)), ((), ()))
+
+
+def moe(tokens, meta, hidden, gate, up, down, n_sp, n_tp, cap):
+    n_inner = math.gcd(n_sp, 4)
+    n_outer = n_sp // n_inner
+    rows, width = tokens.shape
+    chunks = math.gcd(width // 128, 4)
+    part = width // chunks
+    slots = n_inner * cap
     dma = pltpu.SemaphoreType.DMA
+    vmem = pltpu.VMEM
+    blocks = n_outer * chunks
+    low = jnp.bfloat16
     return pl.pallas_call(
-        functools.partial(expert_kernel, n_sp, n_tp, cap, math.gcd(n_sp, 256 // (n_tp * cap))),
-        out_shape=jax.ShapeDtypeStruct(rows.shape, rows.dtype),
-        in_specs=[VMEM] * 4,
+        functools.partial(moe_kernel, n_outer, n_inner, n_tp, chunks),
+        out_shape=jax.ShapeDtypeStruct((rows, width), low),
+        in_specs=[VMEM] * 6,
         out_specs=VMEM,
         scratch_shapes=[
-            pltpu.VMEM((n_sp * n_tp * cap, width), rows.dtype),
-            pltpu.VMEM((n_sp * n_tp * cap, width), rows.dtype),
-            pltpu.VMEM((n_sp * (n_tp - 1) * cap, width), rows.dtype),
-            pltpu.VMEM(rows.shape, rows.dtype),
-            dma((n_sp - 1 + n_sp * (n_tp - 1),)),
-            dma((n_sp * n_tp,)),
-            dma((n_sp * (n_tp - 1),)),
-            dma((n_sp * (n_tp - 1),)),
-            dma((n_sp - 1,)),
-            dma((n_sp,)),
-            dma((1,)),
+            vmem((n_outer, chunks, rows, part), low),
+            vmem((n_outer,) + meta.shape, meta.dtype),
+            vmem((n_outer, chunks, slots, part), low),
+            vmem((n_outer, chunks, slots, part), low),
+            vmem((n_outer, chunks, slots, part), low),
+            vmem((n_outer, chunks, slots, part), low),
+            vmem((n_outer, chunks, rows, part), low),
+            vmem((n_outer + 1, chunks, rows, part), low),
+            vmem((n_tp - 1,) + gate.shape, low),
+            vmem((n_tp - 1,) + up.shape, low),
+            vmem((n_tp - 1,) + down.shape, low),
+            dma((n_outer - 1,)),
+            dma((n_outer,)),
+            dma((blocks,)),
+            dma((blocks,)),
+            dma((blocks,)),
+            dma((blocks * n_inner,)),
+            dma((blocks * n_inner,)),
+            dma((blocks * n_inner,)),
+            dma((blocks * n_inner,)),
+            dma((blocks,)),
+            dma((blocks + chunks,)),
+            dma((3 * (n_tp - 1),)),
+            dma((3 * (n_tp - 1),)),
         ],
-        compiler_params=pltpu.CompilerParams(collective_id=1, has_side_effects=True),
-        name="expert_rows",
-    )(rows, gate, up, down)
+        compiler_params=pltpu.CompilerParams(
+            collective_id=1, has_side_effects=True, vmem_limit_bytes=67043328
+        ),
+        name="experts",
+    )(tokens, meta, hidden, gate, up, down)
 
 
 def heads_kernel(n_tp, own_ref, out_ref, send_sem, recv_sem, local_sem):
@@ -476,29 +699,19 @@
     capacity = max(2, 2 * (row_count * tp_count) // expert_count)
     capacity = -(-capacity // 16) * 16
     top_count = routes.shape[1]
-    width = normed.shape[1]
     flat_expert = routes.reshape(-1)
     onehot = (flat_expert[:, None] == jnp.arange(expert_count, dtype=jnp.int32)[None, :]).astype(
         jnp.int32
     )
     slot_rank = jnp.sum(jnp.cumsum(onehot, axis=0) * onehot, axis=1) - 1
     slot_index = flat_expert * capacity + slot_rank
-    slots = slot_index.reshape(row_count, top_count)
-    slot_count = expert_count * capacity
-    numbers = jnp.arange(slot_count, dtype=jnp.int32)
-    chosen = slots[:, :, None] == numbers[None, None, :]
-    place = jnp.any(chosen, axis=1).astype(jnp.bfloat16)
-    outgoing = lax.dot_general(
-        place, normed, (((0,), (0,)), ((), ())), preferred_element_type=jnp.float32
-    ).astype(jnp.bfloat16)
-    shares = jnp.sum(jnp.where(chosen, route_weight[:, :, None], 0.0), axis=1)
-    share_high = lax.reduce_precision(shares, 8, 7)
-    share_low = shares - share_high
-    back_rows = expert_rows(outgoing, w_gate[0], w_up[0], w_down[0], sp_count, tp_count)
-    combined = jnp.dot(
-        share_high.astype(jnp.bfloat16), back_rows, preferred_element_type=jnp.float32
-    ) + jnp.dot(share_low.astype(jnp.bfloat16), back_rows, preferred_element_type=jnp.float32)
-    return (hidden_wide + combined).astype(jnp.bfloat16)
+    slots = slot_index.reshape(row_count, top_count).astype(jnp.float32)
+    meta = jnp.concatenate(
+        [slots.T, route_weight.T, jnp.zeros((8 - 2 * top_count, row_count), jnp.float32)], axis=0
+    )
+    return moe(
+        normed, meta, hidden, w_gate[0], w_up[0], w_down[0], sp_count, tp_count, capacity
+    )
 
 
 def solution(mesh):

time: 176 us -> 152 us (0.86)
  the two profiles are of different devices: /device:TPU:16 before, /device:TPU:0 now
where the time goes in v1:
time: 152 us
  Pallas kernels  134 us (88%)
  local copies, waits for them, and re-layouts  7.47 us (5%)
  other arithmetic  5.47 us (4%)
  matrix products  4.44 us (3%)
    pallas_call x1, Pallas kernels, moe(): pl.pallas_call(functools.partial(moe_kernel, n_outer, n_inner, n_tp, chun...  95.9 us
    pallas_call x1, Pallas kernels, gather_rows(): pl.pallas_call(functools.partial(gather_kernel, n_sp, n_tp, inner), out_s...  30.1 us
    unnamed x17, local copies, waits for them, and re-layouts  5.55 us
    pallas_call x1, Pallas kernels, attention(): pl.pallas_call(functools.partial(attention_kernel, key_block, latent_widt...  5.14 us
    pallas_call x1, Pallas kernels, swap_heads(): pl.pallas_call(functools.partial(heads_kernel, n_tp), out_shape=jax.Shape...  3.09 us

profile of v1, /device:TPU:0, one launch (start us, length us, event | category | flops | bytes accessed | tf_op | source)
XLA Modules:
  0.0 151.7 jit_solution(2633236100768791813)
XLA Ops:
  0.0 0.0 copy-start.2
  0.0 0.2 multiply_cosine_fusion.1
  0.2 1.0 copy.28
  1.3 0.1 pad.10.clone
  1.4 1.1 copy.27
  2.5 0.9 maximum_bitcast_fusion.query_ref
  3.4 0.8 copy.29
  4.2 0.3 fusion.17
  4.6 0.1 pad.6.clone
  4.6 1.6 %maximum_maximum_fusion.own_ref = bf16[128,384]{1,0:T(8,128)(2,1)} fusion(bf16[128,32]{1,0:T(8,128)(2,1)S(1)} %get-tuple-element.8, bf16[128,32]{1,0:T(8,128)(2,1)S(1)} %get-tuple-element.7, bf16[128,256]{1,0:T(8,128)(2,1)} %param.17, bf16[384]{0:T(512)(128)(2,1)S(1)} %pad.6.clone), kind=kLoop, calls=%fused_computation.18 | loop fusion | flops 393216 | bytes 180992 | tf_op jit(solution)/shard_map/concatenate | solution.py:666
  6.2 30.1 %gather_rows.1 = bf16[32,128,384]{2,1,0:T(8,128)(2,1)} custom-call(bf16[128,384]{1,0:T(8,128)(2,1)} %maximum_maximum_fusion.own_ref), custom_call_target="tpu_custom_call" | custom-call | tf_op jit(solution)/shard_map/gather_rows/pallas_call | solution.py:123
  36.3 0.0 copy-done.2
  36.3 0.8 copy.31
  37.1 0.0 copy-start.1
  37.1 5.1 %attention.1.own_ref = bf16[256,512]{1,0:T(8,128)(2,1)} custom-call(s32[1]{0:T(128)} %bitcast.base_ref, bf16[4,256,256]{2,1,0:T(8,128)(2,1)} %maximum_bitcast_fusion.query_ref, bf16[4096,384]{1,0:T(8,128)(2,1)} %bitcast.36, bf16[256,512]{1,0:T(8,128)(2,1)} %key_up_ref.1, bf16[512,256]{1,0:T(8,128)(2,1)} %bitcast.39), custom_call_target="tpu_custom_call" | custom-call | tf_op jit(solution)/shard_map/attention/pallas_call | solution.py:620
  42.3 0.0 copy-start.3
  42.3 3.1 %swap_heads.1 = bf16[2,128,512]{2,1,0:T(8,128)(2,1)} custom-call(bf16[256,512]{1,0:T(8,128)(2,1)} %attention.1.own_ref), custom_call_target="tpu_custom_call" | custom-call | tf_op jit(solution)/shard_map/swap_heads/pallas_call | solution.py:540
  45.4 0.0 copy-start.4
  45.4 0.0 copy-start.5
  45.4 2.1 %fusion.3 = f32[128,2048]{1,0:T(8,128)S(1)} fusion(bf16[1024,2048]{1,0:T(8,128)(2,1)} %param.21, bf16[2,128,512]{2,1,0:T(8,128)(2,1)} %swap_heads.1), kind=kOutput, calls=%fused_computation.4 | convolution fusion | flops 268435456 | bytes 3276800 | tf_op jit(solution)/shard_map/dot_general | solution.py:686
  47.5 0.0 copy-done.1
  47.5 2.3 %fusion.5 = (f32[128]{0:T(128)S(1)}, bf16[128,2048]{1,0:T(8,128)(2,1)S(1)}) fusion(f32[128,2048]{1,0:T(8,128)S(1)} %fusion.3, bf16[1024,2048]{1,0:T(8,128)(2,1)} %param.21, bf16[2,128,512]{2,1,0:T(8,128)(2,1)} %swap_heads.1, bf16[128,2048]{1,0:T(8,128)(2,1)S(1)} %copy-done.1), kind=kOutput, calls=%fused_computation.8 | convolution fusion | flops 270270336 | bytes 4325888 | tf_op jit(solution)/shard_map/dot_general | solution.py:688
  49.9 0.0 copy-start
  49.9 0.8 copy-done
  50.7 0.0 copy-done.3
  50.7 1.0 fusion.7.tok_ref
  51.7 0.0 copy-done.4
  51.7 0.1 copy.32
  51.8 0.1 eq.29
  51.9 0.6 reduce-window.6
  52.5 0.2 slice_reduce_fusion
  52.7 0.1 eq.25
  52.9 0.1 fusion.21
  53.0 0.1 sub.15
  53.1 0.1 copy.35
  53.2 0.1 pad.2.clone
  53.3 0.0 copy-done.5
  53.3 0.7 maximum_maximum_fusion.1.meta_ref
  54.0 95.9 %experts.1 = bf16[128,2048]{1,0:T(8,128)(2,1)} custom-call(bf16[128,2048]{1,0:T(8,128)(2,1)} %fusion.7.tok_ref, f32[8,128]{1,0:T(8,128)} %maximum_maximum_fusion.1.meta_ref, bf16[128,2048]{1,0:T(8,128)(2,1)} %copy-done, bf16[2048,256]{1,0:T(8,128)(2,1)} %bitcast.40, bf16[2048,256]{1,0:T(8,128)(2,1)} %bitcast.41, bf16[256,2048]{1,0:T(8,128)(2,1)} %bitcast.42), custom_call_target="tpu_custom_call" | custom-call | tf_op jit(solution)/shard_map/experts/pallas_call | solution.py:479
  149.9 1.9 %copy.39 = bf16[128,2048]{1,0:T(8,128)(2,1)} copy(bf16[128,2048]{1,0:T(8,128)(2,1)} %experts.1) | data formatting | bytes 1048576
  (13 shorter events, 0.1 us)
Async XLA Ops:
  0.0 36.3 %copy-start.2 = (bf16[256,512]{1,0:T(8,128)(2,1)S(1)}, bf16[256,512]{1,0:T(8,128)(2,1)}, u32[]{:S(2)}) copy-start(bf16[256,512]{1,0:T(8,128)(2,1)} %param.20) | copy-start | bytes 786436
  37.1 10.4 %copy-start.1 = (bf16[128,2048]{1,0:T(8,128)(2,1)S(1)}, bf16[128,2048]{1,0:T(8,128)(2,1)}, u32[]{:S(2)}) copy-start(bf16[128,2048]{1,0:T(8,128)(2,1)} %param.14) | copy-start | bytes 1572868
  42.3 8.4 %copy-start.3 = (f32[2048]{0:T(1024)S(1)}, f32[2048]{0:T(1024)}, u32[]{:S(2)}) copy-start(f32[2048]{0:T(1024)} %param.22) | copy-start | bytes 24580
  45.4 6.3 %copy-start.4 = (s32[128,2]{0,1:T(2,128)S(1)}, s32[128,2]{0,1:T(2,128)}, u32[]{:S(2)}) copy-start(s32[128,2]{0,1:T(2,128)} %param.23) | copy-start | bytes 3076
  45.4 7.9 %copy-start.5 = (f32[128,2]{0,1:T(2,128)S(1)}, f32[128,2]{0,1:T(2,128)}, u32[]{:S(2)}) copy-start(f32[128,2]{0,1:T(2,128)} %param.24) | copy-start | bytes 3076
  49.9 0.8 copy-start

commit v2 on v1

--- a/solution.py
+++ b/solution.py
@@ -19,23 +19,6 @@
 NEG_LARGE = -1e30
 
 
-def rotary(values, positions):
-    half_width = values.shape[-1] // 2
-    inverse = ROPE_BASE ** (-2.0 * jnp.arange(half_width, dtype=jnp.float32) / values.shape[-1])
-    angles = positions.astype(jnp.float32)[:, None] * inverse[None, :]
-    cosine = jnp.cos(angles)
-    sine_part = jnp.sin(angles)
-    if values.ndim == 3:
-        cosine = cosine[:, None, :]
-        sine_part = sine_part[:, None, :]
-    first_half = values[..., :half_width]
-    second = values[..., half_width:]
-    return jnp.concatenate(
-        [first_half * cosine - second * sine_part, second * cosine + first_half * sine_part],
-        axis=-1,
-    )
-
-
 MESH = pl.DeviceIdType.MESH
 VMEM = pl.BlockSpec(memory_space=pltpu.VMEM)
 
@@ -47,92 +30,389 @@
     pl.semaphore_wait(barrier, len(peers))
 
 
-def far_first(count):
-    return sorted(range(1, count), key=lambda step: abs(2 * step - count))
-
-
-def send(source, target, send_sem, recv_sem, peer):
-    copy = pltpu.make_async_remote_copy(
-        src_ref=source,
-        dst_ref=target,
-        send_sem=send_sem,
-        recv_sem=recv_sem,
-        device_id=peer,
-        device_id_type=MESH,
-    )
-    copy.start()
-    return copy
-
-
 def arrived(block, semaphore):
     pltpu.make_async_copy(block, block, semaphore).wait()
 
 
-def gather_kernel(n_sp, n_tp, inner, own_ref, out_ref, send_sem, recv_sem, local_sem):
+def attend_kernel(
+    n_outer,
+    n_inner,
+    n_tp,
+    table_ref,
+    nope_ref,
+    rope_ref,
+    latent_ref,
+    key_rope_ref,
+    key_up_ref,
+    value_up_ref,
+    residual_ref,
+    gain_ref,
+    proj_hbm,
+    hidden_ref,
+    normed_ref,
+    kv_ref,
+    query_ref,
+    value_ref,
+    max_ref,
+    sum_ref,
+    acc_ref,
+    own_ref,
+    heads_ref,
+    proj_ref,
+    plane_send,
+    mate_send,
+    twin_send,
+    kv_recv,
+    heads_send,
+    heads_recv,
+    proj_sem,
+):
     sp, tp = lax.axis_index("sp"), lax.axis_index("tp")
-    outer = n_sp // inner
-    group, member = sp // inner, sp % inner
-
-    def column(step):
-        return ((group + step) % outer) * inner + member
-
-    def mate(step):
-        return group * inner + (member + step) % inner
-
-    others = [(column(step), tp) for step in far_first(outer)]
-    mates = [(mate(step), tp) for step in range(1, inner)]
-    twins = [(sp, (tp + step) % n_tp) for step in range(1, n_tp)]
-    greet(others + mates + twins)
-    copies = []
-
-    def push(source, block, peers):
-        for peer in peers:
-            copies.append(
-                send(
-                    source, out_ref.at[block], send_sem.at[len(copies)], recv_sem.at[block], peer
-                )
+    group, member = sp // n_inner, sp % n_inner
+    queries = nope_ref.shape[0]
+    rows, latent_width = latent_ref.shape
+    heads = nope_ref.shape[1] // QK_NOPE
+    packed = rows // (latent_width // QK_ROPE)
+    scale = (QK_NOPE + QK_ROPE) ** (-0.5) * math.log2(math.e)
+    twins = [(tp + hop) % n_tp for hop in range(1, n_tp)]
+    mates = [(member + step) % n_inner for step in range(n_inner)]
+
+    load = pltpu.make_async_copy(proj_hbm, proj_ref, proj_sem)
+    load.start()
+
+    def copy(source, target, send_sem, recv_sem, peer):
+        return pltpu.make_async_remote_copy(
+            src_ref=source,
+            dst_ref=target,
+            send_sem=send_sem,
+            recv_sem=recv_sem,
+            device_id=peer,
+            device_id_type=MESH,
+        )
+
+    def kv_copy(block, send_sem, peer):
+        ref = kv_ref.at[block, tp]
+        return copy(ref, ref, send_sem, kv_recv.at[block * n_tp + tp], peer)
+
+    def plane_copy(step):
+        return kv_copy(sp, plane_send.at[step], ((group + step) * n_inner + member, tp))
+
+    def mate_copy(distance, step):
+        return kv_copy(
+            (group - distance) * n_inner + member,
+            mate_send.at[distance * n_inner + step],
+            (group * n_inner + mates[step], tp),
+        )
+
+    def twin_copies(block):
+        return [
+            kv_copy(block, twin_send.at[block * (n_tp - 1) + hop], (sp, twin))
+            for hop, twin in enumerate(twins)
+        ]
+
+    def landed(block, core):
+        arrived(kv_ref.at[block, core], kv_recv.at[block * n_tp + core])
+
+    lane = lax.broadcasted_iota(jnp.int32, (1, 2 * QK_ROPE), 1)
+    early = lane % QK_ROPE < QK_ROPE // 2
+
+    def rotated(values, first):
+        where = pl.ds(pl.multiple_of(first, values.shape[0]), values.shape[0])
+        values = values.astype(jnp.float32)
+        swapped = jnp.where(
+            early,
+            pltpu.roll(values, 2 * QK_ROPE - QK_ROPE // 2, 1),
+            pltpu.roll(values, QK_ROPE // 2, 1),
+        )
+        return values * table_ref[0, where] + swapped * table_ref[1, where]
+
+    wide_rope = jnp.concatenate([key_rope_ref[...]] * 2, axis=1)
+    key_rot = rotated(wide_rope, tp * rows)
+    kv_ref[sp, tp, :rows] = latent_ref[...]
+    for pair in range(latent_width // (2 * QK_ROPE)):
+        low = key_rot[(2 * pair) * packed : (2 * pair + 1) * packed]
+        high = key_rot[(2 * pair + 1) * packed : (2 * pair + 2) * packed]
+        kv_ref[sp, tp, rows:, pair * 2 * QK_ROPE : (pair + 1) * 2 * QK_ROPE] = jnp.where(
+            lane < QK_ROPE, low, high
+        ).astype(jnp.bfloat16)
+
+    planes = [((group + step) % n_outer * n_inner + member, tp) for step in range(1, n_outer)]
+    greet(
+        planes
+        + [(group * n_inner + mate, tp) for mate in mates[1:]]
+        + [(sp, twin) for twin in twins]
+    )
+
+    for item in twin_copies(sp):
+        item.start()
+    for step in range(1, max(n_inner, n_outer)):
+        if step < n_outer:
+
+            @pl.when(group + step < n_outer)
+            def _():
+                plane_copy(step).start()
+
+        if step < n_inner:
+
+            @pl.when(mates[step] > member)
+            def _():
+                mate_copy(0, step).start()
+
+    for pair in range(0, heads, 2):
+        both = rotated(rope_ref[:, pair * QK_ROPE : (pair + 2) * QK_ROPE], 0).T
+        for head in (pair, pair + 1):
+            columns = slice(head * QK_NOPE, (head + 1) * QK_NOPE)
+            query_ref[head, :QK_NOPE] = nope_ref[:, columns].astype(jnp.float32).T.astype(
+                jnp.bfloat16
             )
-
-    mine = sp * n_tp + tp
-    keep = pltpu.make_async_copy(own_ref, out_ref.at[mine], local_sem)
-    keep.start()
-    push(own_ref, mine, others + mates + twins)
-    for step in sorted(range(1, outer), key=lambda step: min(step, outer - step)):
-        block = column(step) * n_tp + tp
-        arrived(out_ref.at[block], recv_sem.at[block])
-        push(out_ref.at[block], block, mates + twins)
-    for step in range(outer):
-        for hop in range(1, inner):
-            source = ((group + step) % outer) * inner + (member + hop) % inner
-            block = source * n_tp + tp
-            arrived(out_ref.at[block], recv_sem.at[block])
-            push(out_ref.at[block], block, twins)
-    for twin in twins:
-        for source in range(n_sp):
-            block = source * n_tp + twin[1]
-            arrived(out_ref.at[block], recv_sem.at[block])
-    keep.wait()
-    for copy in copies:
-        copy.wait_send()
-
-
-def gather_rows(own, n_sp, n_tp):
-    inner = math.gcd(n_sp, 4)
-    outer = n_sp // inner
-    sends = (outer - 1) + outer * (inner - 1) + n_sp * (n_tp - 1)
+            query_ref[head, QK_NOPE : QK_NOPE + QK_ROPE] = both[
+                (head - pair) * QK_ROPE : (head - pair + 1) * QK_ROPE
+            ].astype(jnp.bfloat16)
+            query_ref[head, QK_NOPE + QK_ROPE :] = jnp.zeros(
+                (QK_ROPE, queries), jnp.bfloat16
+            )
+    value_ref[...] = value_up_ref[...].astype(jnp.float32).T.astype(jnp.bfloat16)
+
+    def attend(blocks, own):
+        latents, rots = [], []
+        for block in blocks:
+            for core in range(n_tp):
+                latents.append(kv_ref[block, core, :rows])
+                for pair in range(latent_width // (2 * QK_ROPE)):
+                    part = kv_ref[
+                        block, core, rows:, pair * 2 * QK_ROPE : (pair + 1) * 2 * QK_ROPE
+                    ].astype(jnp.float32)
+                    rots.append(part.astype(jnp.bfloat16))
+                    rots.append(pltpu.roll(part, QK_ROPE, 1).astype(jnp.bfloat16))
+        latent = jnp.concatenate(latents, axis=0)
+        rot = jnp.concatenate(rots, axis=0)
+        count = latent.shape[0]
+        keys = jnp.dot(latent, key_up_ref[...], preferred_element_type=jnp.float32).astype(
+            jnp.bfloat16
+        )
+        values = lax.dot_general(
+            value_ref[...], latent, NT, preferred_element_type=jnp.float32
+        ).astype(jnp.bfloat16)
+        if own:
+            allowed = (
+                lax.broadcasted_iota(jnp.int32, (count, queries), 0) // SEGMENT
+                <= lax.broadcasted_iota(jnp.int32, (count, queries), 1) // SEGMENT
+            )
+        for head in range(heads):
+            wide = jnp.concatenate([keys[:, head * QK_NOPE : (head + 1) * QK_NOPE], rot], axis=1)
+            scores = jnp.dot(wide, query_ref[head], preferred_element_type=jnp.float32)
+            if own:
+                scores = jnp.where(allowed, scores, NEG_LARGE)
+            new_max = jnp.max(scores, axis=0, keepdims=True)
+            if not own:
+                old_max = max_ref[head]
+                new_max = jnp.maximum(old_max, new_max)
+                shrink = jnp.exp2((old_max - new_max) * scale)
+            weights = jnp.exp2((scores - new_max) * scale)
+            total = jnp.sum(weights, axis=0, keepdims=True)
+            product = jnp.dot(
+                values[head * V_DIM : (head + 1) * V_DIM],
+                weights.astype(jnp.bfloat16),
+                preferred_element_type=jnp.float32,
+            )
+            max_ref[head] = new_max
+            if own:
+                sum_ref[head] = total
+                acc_ref[head] = product
+            else:
+                sum_ref[head] = sum_ref[head] * shrink + total
+                acc_ref[head] = acc_ref[head] * shrink + product
+
+    def from_plane(distance):
+        block = (group - distance) * n_inner + member
+        landed(block, tp)
+        for step in range(1, n_inner):
+            mate_copy(distance, step).start()
+        for item in twin_copies(block):
+            item.start()
+
+    def from_mate(distance, step):
+        block = (group - distance) * n_inner + mates[step]
+        landed(block, tp)
+        for item in twin_copies(block):
+            item.start()
+
+    def ready(distance, step):
+        block = (group - distance) * n_inner + mates[step]
+        for twin in twins:
+            landed(block, twin)
+        return block
+
+    attend([ready(0, 0)], True)
+
+    @pl.when(group >= 1)
+    def _():
+        from_plane(1)
+
+    for step in range(1, n_inner):
+
+        @pl.when(mates[step] < member)
+        def _():
+            from_mate(0, step)
+
+    @pl.when(group >= 2)
+    def _():
+        from_plane(2)
+
+    def inside(step, carry):
+        mate = (member + step) % n_inner
+
+        @pl.when(mate < member)
+        def _():
+            block = group * n_inner + mate
+            for twin in twins:
+                landed(block, twin)
+            attend([block], False)
+
+        return carry
+
+    lax.fori_loop(1, n_inner, inside, 0)
+
+    def outside(distance, carry):
+        @pl.when(distance + 2 <= group)
+        def _():
+            from_plane(distance + 2)
+
+        unit = 2 if n_inner % 2 == 0 else 1
+        for first in range(0, n_inner, unit):
+            for step in range(first, first + unit):
+                if step > 0:
+                    from_mate(distance, step)
+            attend([ready(distance, step) for step in range(first, first + unit)], False)
+        return carry
+
+    lax.fori_loop(1, group + 1, outside, 0)
+
+    def heads_copy(hop):
+        return copy(
+            own_ref.at[pl.ds(pl.multiple_of(twins[hop] * rows, rows), rows)],
+            heads_ref.at[hop],
+            heads_send.at[hop],
+            heads_recv.at[hop],
+            (sp, twins[hop]),
+        )
+
+    for head in range(heads):
+        own_ref[:, head * V_DIM : (head + 1) * V_DIM] = (
+            (acc_ref[head] / sum_ref[head]).T.astype(own_ref.dtype)
+        )
+    for hop in range(n_tp - 1):
+        heads_copy(hop).start()
+    load.wait()
+    depth = heads * V_DIM
+    width = residual_ref.shape[1]
+    part = width // math.gcd(width // 128, 4)
+
+    def proj(core, columns):
+        return proj_ref[pl.ds(pl.multiple_of(core * depth, depth), depth), columns]
+
+    mine = own_ref[pl.ds(pl.multiple_of(tp * rows, rows), rows)]
+    spans = [slice(first, first + part) for first in range(0, width, part)]
+    sums = []
+    for columns in spans:
+        sums.append(
+            residual_ref[:, columns].astype(jnp.float32)
+            + jnp.dot(mine, proj(tp, columns), preferred_element_type=jnp.float32)
+        )
+    for hop in range(n_tp - 1):
+        arrived(heads_ref.at[hop], heads_recv.at[hop])
+        for number, columns in enumerate(spans):
+            sums[number] = sums[number] + jnp.dot(
+                heads_ref[hop], proj((tp + n_tp - hop - 1) % n_tp, columns),
+                preferred_element_type=jnp.float32,
+            )
+    square = jnp.zeros((rows, 1), jnp.float32)
+    for number, columns in enumerate(spans):
+        hidden = sums[number].astype(jnp.bfloat16)
+        hidden_ref[:, columns] = hidden
+        hidden = hidden.astype(jnp.float32)
+        square = square + jnp.sum(hidden * hidden, axis=1, keepdims=True)
+    factor = lax.rsqrt(square / width + EPSILON)
+    for columns in spans:
+        normed_ref[:, columns] = (
+            hidden_ref[:, columns].astype(jnp.float32) * factor * gain_ref[:, columns]
+        ).astype(jnp.bfloat16)
+
+    for hop in range(n_tp - 1):
+        heads_copy(hop).wait_send()
+    for item in twin_copies(sp):
+        item.wait_send()
+    for step in range(1, n_outer):
+
+        @pl.when(group + step < n_outer)
+        def _():
+            plane_copy(step).wait_send()
+
+    for step in range(1, n_inner):
+
+        @pl.when(mates[step] > member)
+        def _():
+            mate_copy(0, step).wait_send()
+
+        @pl.when(mates[step] < member)
+        def _():
+            for item in twin_copies(group * n_inner + mates[step]):
+                item.wait_send()
+
+    def drain(distance, carry):
+        for step in range(n_inner):
+            if step > 0:
+                mate_copy(distance, step).wait_send()
+            for item in twin_copies((group - distance) * n_inner + mates[step]):
+                item.wait_send()
+        return carry
+
+    lax.fori_loop(1, group + 1, drain, 0)
+
+
+NT = (((1,), (1,)), ((), ()))
+
+
+def attend(
+    table, nope, rope, latent, key_rope, key_up, value_up, residual, gain, proj, n_sp, n_tp
+):
+    n_inner = math.gcd(n_sp, 4)
+    n_outer = n_sp // n_inner
+    queries = nope.shape[0]
+    heads = nope.shape[1] // QK_NOPE
+    rows, latent_width = latent.shape
+    packed = rows // (latent_width // QK_ROPE)
+    dma = pltpu.SemaphoreType.DMA
+    vmem = pltpu.VMEM
+    low, wide = jnp.bfloat16, jnp.float32
     return pl.pallas_call(
-        functools.partial(gather_kernel, n_sp, n_tp, inner),
-        out_shape=jax.ShapeDtypeStruct((n_sp * n_tp,) + own.shape, own.dtype),
-        in_specs=[VMEM],
-        out_specs=VMEM,
+        functools.partial(attend_kernel, n_outer, n_inner, n_tp),
+        out_shape=[jax.ShapeDtypeStruct(residual.shape, low)] * 2,
+        in_specs=[VMEM] * 9 + [pl.BlockSpec(memory_space=pl.ANY)],
+        out_specs=[VMEM] * 2,
         scratch_shapes=[
-            pltpu.SemaphoreType.DMA((sends,)),
-            pltpu.SemaphoreType.DMA((n_sp * n_tp,)),
-            pltpu.SemaphoreType.DMA,
+            vmem((n_sp, n_tp, rows + packed, latent_width), low),
+            vmem((heads, QK_NOPE + 2 * QK_ROPE, queries), low),
+            vmem((heads * V_DIM, latent_width), low),
+            vmem((heads, 1, queries), wide),
+            vmem((heads, 1, queries), wide),
+            vmem((heads, V_DIM, queries), wide),
+            vmem((queries, heads * V_DIM), low),
+            vmem((n_tp - 1, rows, heads * V_DIM), low),
+            vmem(proj.shape, low),
+            dma((n_outer,)),
+            dma((n_sp,)),
+            dma((n_sp * (n_tp - 1),)),
+            dma((n_sp * n_tp,)),
+            dma((n_tp - 1,)),
+            dma((n_tp - 1,)),
+            dma,
         ],
-        compiler_params=pltpu.CompilerParams(collective_id=0, has_side_effects=True),
-        name="gather_rows",
-    )(own)
+        compiler_params=pltpu.CompilerParams(
+            collective_id=0, has_side_effects=True, vmem_limit_bytes=48 * 2**20
+        ),
+        name="attend",
+    )(table, nope, rope, latent, key_rope, key_up, value_up, residual, gain, proj)
 
 
 def moe_kernel(
@@ -514,123 +794,6 @@
     )(tokens, meta, hidden, gate, up, down)
 
 
-def heads_kernel(n_tp, own_ref, out_ref, send_sem, recv_sem, local_sem):
-    sp, tp = lax.axis_index("sp"), lax.axis_index("tp")
-    twins = [(sp, (tp + hop) % n_tp) for hop in range(1, n_tp)]
-    greet(twins)
-    rows = out_ref.shape[1]
-
-    def part(core):
-        return own_ref.at[pl.ds(pl.multiple_of(core * rows, rows), rows)]
-
-    copies = [
-        send(part(twin[1]), out_ref.at[tp], send_sem.at[hop], recv_sem.at[tp], twin)
-        for hop, twin in enumerate(twins)
-    ]
-    keep = pltpu.make_async_copy(part(tp), out_ref.at[tp], local_sem)
-    keep.start()
-    for twin in twins:
-        arrived(out_ref.at[twin[1]], recv_sem.at[twin[1]])
-    keep.wait()
-    for copy in copies:
-        copy.wait_send()
-
-
-def swap_heads(own, n_tp):
-    return pl.pallas_call(
-        functools.partial(heads_kernel, n_tp),
-        out_shape=jax.ShapeDtypeStruct((n_tp, own.shape[0] // n_tp, own.shape[1]), own.dtype),
-        in_specs=[VMEM],
-        out_specs=VMEM,
-        scratch_shapes=[
-            pltpu.SemaphoreType.DMA((n_tp - 1,)),
-            pltpu.SemaphoreType.DMA((n_tp,)),
-            pltpu.SemaphoreType.DMA,
-        ],
-        compiler_params=pltpu.CompilerParams(collective_id=2, has_side_effects=True),
-        name="swap_heads",
-    )(own)
-
-
-NT = (((1,), (1,)), ((), ()))
-
-
-def attention_kernel(
-    key_block, latent_width, heads, base_ref, query_ref, kv_ref, key_up_ref, value_up_ref, out_ref, max_ref, sum_ref, acc_ref
-):
-    first = base_ref[0]
-    queries = query_ref.shape[2]
-    scale = (QK_NOPE + QK_ROPE) ** (-0.5) * math.log2(math.e)
-    max_ref[...] = jnp.full_like(max_ref, NEG_LARGE)
-    sum_ref[...] = jnp.zeros_like(sum_ref)
-    acc_ref[...] = jnp.zeros_like(acc_ref)
-
-    def block(start, masked):
-        start = pl.multiple_of(start, key_block)
-        rows = kv_ref[pl.ds(start, key_block), :]
-        latent = rows[:, :latent_width]
-        rot = rows[:, latent_width:]
-        keys = jnp.dot(latent, key_up_ref[...], preferred_element_type=jnp.float32).astype(
-            jnp.bfloat16
-        )
-        values = lax.dot_general(
-            value_up_ref[...], latent, NT, preferred_element_type=jnp.float32
-        ).astype(jnp.bfloat16)
-        if masked:
-            key_segment = (
-                start + lax.broadcasted_iota(jnp.int32, (key_block, queries), 0)
-            ) // SEGMENT
-            query_segment = (
-                first + lax.broadcasted_iota(jnp.int32, (key_block, queries), 1)
-            ) // SEGMENT
-            allowed = key_segment <= query_segment
-        for head in range(heads):
-            wide = jnp.concatenate([keys[:, head * QK_NOPE : (head + 1) * QK_NOPE], rot], axis=1)
-            scores = jnp.dot(wide, query_ref[head], preferred_element_type=jnp.float32)
-            if masked:
-                scores = jnp.where(allowed, scores, NEG_LARGE)
-            old_max = max_ref[head]
-            new_max = jnp.maximum(old_max, jnp.max(scores, axis=0, keepdims=True))
-            weights = jnp.exp2((scores - new_max) * scale)
-            shrink = jnp.exp2((old_max - new_max) * scale)
-            max_ref[head] = new_max
-            sum_ref[head] = sum_ref[head] * shrink + jnp.sum(weights, axis=0, keepdims=True)
-            acc_ref[head] = acc_ref[head] * shrink + jnp.dot(
-                values[head * V_DIM : (head + 1) * V_DIM],
-                weights.astype(jnp.bfloat16),
-                preferred_element_type=jnp.float32,
-            )
-
-    whole = first // key_block
-
-    def body(step, carry):
-        block(step * key_block, False)
-        return carry
-
-    lax.fori_loop(0, whole, body, 0)
-    block(whole * key_block, True)
-    for head in range(heads):
-        out_ref[:, head * V_DIM : (head + 1) * V_DIM] = (
-            (acc_ref[head] / sum_ref[head]).T.astype(out_ref.dtype)
-        )
-
-
-def attention(base, query, kv, key_up, value_up_t, key_block, latent_width):
-    heads, unused, queries = query.shape
-    return pl.pallas_call(
-        functools.partial(attention_kernel, key_block, latent_width, heads),
-        out_shape=jax.ShapeDtypeStruct((queries, heads * V_DIM), jnp.bfloat16),
-        in_specs=[pl.BlockSpec(memory_space=pltpu.SMEM), VMEM, VMEM, VMEM, VMEM],
-        out_specs=VMEM,
-        scratch_shapes=[
-            pltpu.VMEM((heads, 1, queries), jnp.float32),
-            pltpu.VMEM((heads, 1, queries), jnp.float32),
-            pltpu.VMEM((heads, V_DIM, queries), jnp.float32),
-        ],
-        name="attention",
-    )(base, query, kv, key_up, value_up_t)
-
-
 def local(
     residual,
     query_nope,
@@ -649,52 +812,28 @@
 ):
     tp_count = lax.axis_size("tp")
     sp_count = lax.axis_size("sp")
-    tp_index = lax.axis_index("tp")
-    sp_index = lax.axis_index("sp")
     row_count = residual.shape[0]
     tok_dev = query_nope.shape[0]
-    heads_here = query_nope.shape[1] // QK_NOPE
-    query_first = sp_index * tok_dev
-    query_pos = query_first + jnp.arange(tok_dev, dtype=jnp.int32)
-    query_rot = rotary(
-        query_rope.astype(jnp.float32).reshape(tok_dev, heads_here, QK_ROPE), query_pos
-    ).astype(jnp.bfloat16)
-    query_heads = query_nope.reshape(tok_dev, heads_here, QK_NOPE)
-    key_pos = query_first + tp_index * row_count + jnp.arange(row_count, dtype=jnp.int32)
-    key_rot = rotary(key_rope.astype(jnp.float32), key_pos).astype(jnp.bfloat16)
-    width_pad = -(-QK_ROPE // 128) * 128 - QK_ROPE
-    packed = jnp.concatenate(
-        [latent, key_rot, jnp.zeros((row_count, width_pad), jnp.bfloat16)], axis=1
+    half = QK_ROPE // 2
+    inverse = ROPE_BASE ** (-2.0 * jnp.arange(half, dtype=jnp.float32) / QK_ROPE)
+    positions = lax.axis_index("sp") * tok_dev + jnp.arange(tok_dev, dtype=jnp.int32)
+    angles = positions.astype(jnp.float32)[:, None] * jnp.tile(inverse, 4)[None, :]
+    sign = jnp.tile(jnp.repeat(jnp.array([-1.0, 1.0], jnp.float32), half), 2)
+    table = jnp.stack([jnp.cos(angles), jnp.sin(angles) * sign[None, :]])
+    hidden, normed = attend(
+        table,
+        query_nope,
+        query_rope,
+        latent,
+        key_rope,
+        key_up,
+        value_up,
+        residual,
+        norm_gain[None, :],
+        out_proj,
+        sp_count,
+        tp_count,
     )
-    gathered = gather_rows(packed, sp_count, tp_count)
-    kv_rows = gathered.reshape(sp_count * tok_dev, packed.shape[1])
-    query = jnp.concatenate(
-        [query_heads, query_rot, jnp.zeros((tok_dev, heads_here, width_pad), jnp.bfloat16)], axis=2
-    ).transpose(1, 2, 0)
-    key_block = tok_dev * math.gcd(sp_count, 2)
-    attn_out = attention(
-        query_first.astype(jnp.int32).reshape(1),
-        query,
-        kv_rows,
-        key_up,
-        value_up.T,
-        key_block,
-        latent.shape[1],
-    )
-    all_heads = swap_heads(attn_out, tp_count)
-    proj_parts = out_proj.reshape(tp_count, attn_out.shape[1], out_proj.shape[1])
-    projected = jnp.dot(all_heads[0], proj_parts[0], preferred_element_type=jnp.float32)
-    for core in range(1, tp_count):
-        projected = projected + jnp.dot(
-            all_heads[core], proj_parts[core], preferred_element_type=jnp.float32
-        )
-    hidden_wide = residual.astype(jnp.float32) + projected
-    hidden = hidden_wide.astype(jnp.bfloat16)
-    hidden_wide = hidden.astype(jnp.float32)
-    normed = hidden_wide * lax.rsqrt(
-        jnp.mean(hidden_wide * hidden_wide, axis=-1, keepdims=True) + EPSILON
-    )
-    normed = (normed * norm_gain[None, :]).astype(jnp.bfloat16)
     expert_count = lax.axis_size("sp")
     capacity = max(2, 2 * (row_count * tp_count) // expert_count)
     capacity = -(-capacity // 16) * 16

time: 152 us -> 136 us (0.89)
  Pallas kernels: 134 us -> 119 us
  local copies, waits for them, and re-layouts: 7.47 us -> 13.1 us
  matrix products: 4.44 us -> 0 us
  other arithmetic: 5.47 us -> 3.34 us
    pallas_call x3 -> x1, Pallas kernels: 38.3 us -> 11.1 us  [attend(): pl.pallas_call(functools.partial(attend_kernel, n_outer, n_inner, n_tp),...]
    pallas_call x1, Pallas kernels: 95.9 us -> 108 us  [moe(): pl.pallas_call(functools.partial(moe_kernel, n_outer, n_inner, n_tp, chun...]
    unnamed x17 -> x21, local copies, waits for them, and re-layouts: 5.55 us -> 11.4 us
    dot_general x2 -> x0, matrix products: 4.44 us -> none  [the longest x1 2.32 us: local(): jnp.dot(all_heads[core], proj_parts[core], preferred_element_type=jnp.flo...]
    concatenate x1 -> x0, other arithmetic: 1.55 us -> none  [local(): jnp.concatenate([latent, key_rot, jnp.zeros((row_count, width_pad), jnp.b...]
where the time goes in v2:
time: 136 us
  Pallas kernels  119 us (88%)
  local copies, waits for them, and re-layouts  13.1 us (10%)
  other arithmetic  3.34 us (2%)
    pallas_call x1, Pallas kernels, moe(): pl.pallas_call(functools.partial(moe_kernel, n_outer, n_inner, n_tp, chun...  108 us
    unnamed x21, local copies, waits for them, and re-layouts  11.4 us
    pallas_call x1, Pallas kernels, attend(): pl.pallas_call(functools.partial(attend_kernel, n_outer, n_inner, n_tp),...  11.1 us

profile of v2, /device:TPU:0, one launch (start us, length us, event | category | flops | bytes accessed | tf_op | source)
XLA Modules:
  0.0 135.6 jit_solution(16214456416745786348)
XLA Ops:
  0.0 0.1 pad.2.clone
  0.1 0.7 broadcast_in_dim.11
  0.8 0.1 tile.14
  0.9 0.1 mul.64
  1.0 0.1 mul.61
  1.1 0.8 copy.17.key_rope_ref
  1.9 0.8 copy.18
  2.7 0.1 eq.29
  2.8 0.1 eq.25
  3.0 0.6 reduce-window.6
  3.6 0.2 slice_reduce_fusion
  3.8 0.1 fusion.2
  3.9 0.1 sub.7
  4.1 0.1 copy.21
  4.1 0.7 convert_bitcast_fusion
  4.8 1.3 maximum_maximum_fusion.meta_ref
  6.2 0.5 multiply_cosine_fusion
  6.7 0.0 copy-start
  6.8 1.0 copy-done
  7.8 0.0 copy-start.3
  7.8 0.9 copy-done.3
  8.7 0.0 copy-start.4
  8.7 0.9 copy-done.4
  9.7 0.0 copy-start.5
  9.7 0.9 copy-done.5
  10.6 0.0 copy-start.6
  10.6 0.9 copy-done.6
  11.5 0.0 copy-start.7
  11.5 0.8 copy-done.7
  12.4 0.0 copy-start.8
  12.4 0.7 copy-done.8
  13.1 11.1 %attend.1 = (bf16[128,2048]{1,0:T(8,128)(2,1)S(1)}, bf16[128,2048]{1,0:T(8,128)(2,1)S(1)}) custom-call(f32[2,256,128]{2,1,0:T(8,128)S(1)} %pad_maximum_fusion.table_ref, bf16[256,512]{1,0:T(8,128)(2,1)S(1)} %copy-done.3, bf16[256,256]{1,0:T(8,128)(2,1)S(1)} %copy-done.6, bf16[128,256]{1,0:T(8,128)(2,1)S(1)} %copy-done.7, ...), custom_call_target="tpu_custom_call" | custom-call | tf_op jit(solution)/shard_map/attend/pallas_call | solution.py:388
  24.2 0.0 copy-start.1
  24.2 0.8 copy-done.1
  25.0 0.0 copy-start.2
  25.0 0.8 copy-done.2
  25.8 108.0 %experts.1 = bf16[128,2048]{1,0:T(8,128)(2,1)} custom-call(bf16[128,2048]{1,0:T(8,128)(2,1)} %copy-done.2, f32[8,128]{1,0:T(8,128)} %maximum_maximum_fusion.meta_ref, bf16[128,2048]{1,0:T(8,128)(2,1)} %copy-done.1, bf16[2048,256]{1,0:T(8,128)(2,1)} %bitcast.23, bf16[2048,256]{1,0:T(8,128)(2,1)} %bitcast.24, bf16[256,2048]{1,0:T(8,128)(2,1)} %bitcast.25), custom_call_target="tpu_custom_call" | custom-call | tf_op jit(solution)/shard_map/experts/pallas_call | solution.py:759
  133.7 1.9 %copy.25 = bf16[128,2048]{1,0:T(8,128)(2,1)} copy(bf16[128,2048]{1,0:T(8,128)(2,1)} %experts.1) | data formatting | bytes 1048576
  (10 shorter events, 0.1 us)
Async XLA Ops:
  6.7 1.0 copy-start
  7.8 0.9 copy-start.3
  8.7 0.9 copy-start.4
  9.7 0.9 copy-start.5
  10.6 0.9 copy-start.6
  11.5 0.8 copy-start.7
  12.4 0.7 copy-start.8
  24.2 0.8 copy-start.1
  25.0 0.8 copy-start.2

commit v3 on v1

v3 whole, which is shorter than its diff:
```python
import functools
import math

import jax
import jax.numpy as jnp
from jax import lax
from jax.experimental import pallas as pl
from jax.experimental.pallas import tpu as pltpu
from jax.sharding import PartitionSpec as P
import numpy as np

QK_NOPE = 128
QK_ROPE = 64
V_DIM = 128
SEGMENT = 64


EPSILON = 1e-06
ROPE_BASE = 10000.0
NEG_LARGE = -1e30


MESH = pl.DeviceIdType.MESH
VMEM = pl.BlockSpec(memory_space=pltpu.VMEM)


def greet(peers):
    barrier = pltpu.get_barrier_semaphore()
    for peer in peers:
        pl.semaphore_signal(barrier, inc=1, device_id=peer, device_id_type=MESH)
    pl.semaphore_wait(barrier, len(peers))


def arrived(block, semaphore):
    pltpu.make_async_copy(block, block, semaphore).wait()


def layer_kernel(
    n_outer,
    n_inner,
    n_tp,
    chunks,
    cap,
    inverse_hbm,
    routes_hbm,
    share_hbm,
    latent_hbm,
    key_rope_hbm,
    rope_hbm,
    nope_hbm,
    key_up_hbm,
    value_up_hbm,
    gain_hbm,
    residual_hbm,
    proj_hbm,
    gate_hbm,
    up_hbm,
    down_hbm,
    out_ref,
    inverse_ref,
    routes_ref,
    share_ref,
    latent_ref,
    key_rope_ref,
    rope_ref,
    nope_ref,
    key_up_ref,
    value_up_ref,
    gain_ref,
    residual_ref,
    proj_ref,
    gate_ref,
    up_ref,
    down_ref,
    table_ref,
    kv_ref,
    query_ref,
    value_ref,
    max_ref,
    sum_ref,
    acc_ref,
    own_ref,
    heads_ref,
    hidden_ref,
    tok_all,
    meta_ref,
    meta_all,
    disp_ref,
    in_ref,
    back_ref,
    sum_in,
    gate_all,
    up_all,
    down_all,
    load_sem,
    plane_send,
    mate_send,
    twin_send,
    kv_recv,
    heads_send,
    heads_recv,
    meta_send,
    meta_recv,
    above_send,
    below_send,
    tok_recv,
    disp_send,
    disp_recv,
    back_send,
    back_recv,
    sum_send,
    sum_recv,
    weight_send,
    weight_recv,
):
    sp, tp = lax.axis_index("sp"), lax.axis_index("tp")
    group, member = sp // n_inner, sp % n_inner
    queries = nope_ref.shape[0]
    rows, latent_width = latent_ref.shape
    heads = nope_ref.shape[1] // QK_NOPE
    packed = rows // (latent_width // QK_ROPE)
    scale = (QK_NOPE + QK_ROPE) ** (-0.5) * math.log2(math.e)
    width = residual_ref.shape[1] // chunks
    slots = n_inner * cap
    last = n_outer - 1
    has_above, has_below = group < last, group > 0
    cores = [(tp + hop) % n_tp for hop in range(1, n_tp)]
    places = [(member + step) % n_inner for step in range(n_inner)]
    mates = places[1:]
    twins = [(sp, core) for core in cores]

    loads = {}
    for number, (source, target) in enumerate(
        [
            (inverse_hbm, inverse_ref),
            (key_rope_hbm, key_rope_ref),
            (latent_hbm, latent_ref),
            (routes_hbm, routes_ref),
            (share_hbm, share_ref),
            (rope_hbm, rope_ref),
            (nope_hbm, nope_ref),
            (value_up_hbm, value_up_ref),
            (key_up_hbm, key_up_ref),
            (gain_hbm, gain_ref),
            (residual_hbm, residual_ref),
            (proj_hbm, proj_ref),
            (gate_hbm, gate_ref),
            (up_hbm, up_ref),
            (down_hbm, down_ref),
        ]
    ):
        loads[id(target)] = pltpu.make_async_copy(source, target, load_sem.at[number])
        loads[id(target)].start()

    def loaded(*refs):
        for ref in refs:
            loads[id(ref)].wait()

    def at(plane, place):
        return (plane * n_inner + place, tp)

    others = [at((group + step) % n_outer, member) for step in range(1, n_outer)]

    def copy(source, target, send_sem, recv_sem, peer):
        return pltpu.make_async_remote_copy(
            src_ref=source,
            dst_ref=target,
            send_sem=send_sem,
            recv_sem=recv_sem,
            device_id=peer,
            device_id_type=MESH,
        )

    def span(place):
        return pl.ds(pl.multiple_of(place * cap, cap), cap)

    def kv_copy(block, send_sem, peer):
        ref = kv_ref.at[block, tp]
        return copy(ref, ref, send_sem, kv_recv.at[block * n_tp + tp], peer)

    def plane_copy_kv(step):
        return kv_copy(sp, plane_send.at[step], at(group + step, member))

    def mate_copy(distance, step):
        return kv_copy(
            (group - distance) * n_inner + member,
            mate_send.at[distance * n_inner + step],
            at(group, places[step]),
        )

    def twin_copies(block):
        return [
            kv_copy(block, twin_send.at[block * (n_tp - 1) + hop], twin)
            for hop, twin in enumerate(twins)
        ]

    def landed(block, core):
        arrived(kv_ref.at[block, core], kv_recv.at[block * n_tp + core])

    def meta_copy(step):
        return copy(
            meta_ref, meta_all.at[group], meta_send.at[step], meta_recv.at[group], others[step]
        )

    def relay(block, chunk, upward):
        sems = above_send if upward else below_send
        ref = tok_all.at[block, chunk]
        number = block * chunks + chunk
        peer = at(group + 1 if upward else group - 1, member)
        return copy(ref, ref, sems.at[number], tok_recv.at[number], peer)

    def plane_copy(source, target, send_sem, recv_sem, block, chunk, mate):
        number = (block * chunks + chunk) * n_inner
        return copy(
            source.at[block, chunk, span(mate)],
            target.at[block, chunk, span(member)],
            send_sem.at[number + mate],
            recv_sem.at[number + member],
            at(group, mate),
        )

    def disp_copy(block, chunk, mate):
        return plane_copy(disp_ref, in_ref, disp_send, disp_recv, block, chunk, mate)

    def back_copy(block, chunk, mate):
        return plane_copy(disp_ref, back_ref, back_send, back_recv, block, chunk, mate)

    def plane_arrived(target, recv_sem, block, chunk):
        for mate in mates:
            arrived(
                target.at[block, chunk, span(mate)],
                recv_sem.at[(block * chunks + chunk) * n_inner + mate],
            )

    def sum_copy(block, chunk, downward):
        slot = jnp.where(downward | (block != group + 1), block, n_outer)
        peer = at(jnp.where(downward, group - 1, group + 1), member)
        return copy(
            tok_all.at[block, chunk],
            sum_in.at[slot, chunk],
            sum_send.at[block * chunks + chunk],
            sum_recv.at[slot * chunks + chunk],
            peer,
        )

    weights = [(gate_hbm, gate_all), (up_hbm, up_all), (down_hbm, down_all)]

    def weight_copies():
        for hop, twin in enumerate(twins):
            for number, (own, everyone) in enumerate(weights):
                slot = hop * 3 + number
                yield copy(
                    own, everyone.at[hop], weight_send.at[slot], weight_recv.at[slot], twin
                )

    first_slot = (group * slots).astype(jnp.float32)

    def named(block):
        numbers = first_slot + lax.broadcasted_iota(jnp.int32, (slots, rows), 0).astype(
            jnp.float32
        )
        meta = meta_all[block]
        return meta[0:1] == numbers, meta[1:2] == numbers, meta

    def scatter(block, chunk):
        one, two, unused = named(block)
        place = jnp.where(one | two, 1.0, 0.0).astype(jnp.bfloat16)
        disp_ref[block, chunk] = jnp.dot(
            place, tok_all[block, chunk], preferred_element_type=jnp.float32
        ).astype(jnp.bfloat16)
        for mate in mates:
            disp_copy(block, chunk, mate).start()
        in_ref[block, chunk, span(member)] = disp_ref[block, chunk, span(member)]

    def expert(block):
        for chunk in range(chunks):
            plane_arrived(in_ref, disp_recv, block, chunk)
        inputs = jnp.concatenate([in_ref[block, chunk] for chunk in range(chunks)], axis=1)
        halves = []
        for hop in range(n_tp):
            gate_half = gate_ref[...] if hop == 0 else gate_all[hop - 1]
            up_half = up_ref[...] if hop == 0 else up_all[hop - 1]
            gate = jnp.dot(inputs, gate_half, preferred_element_type=jnp.float32)
            up = jnp.dot(inputs, up_half, preferred_element_type=jnp.float32)
            halves.append((gate / (1.0 + jnp.exp(-gate)) * up).astype(jnp.bfloat16))
        for chunk in range(chunks):
            columns = slice(chunk * width, (chunk + 1) * width)
            made = jnp.dot(halves[0], down_ref[:, columns], preferred_element_type=jnp.float32)
            for hop in range(1, n_tp):
                made = made + jnp.dot(
                    halves[hop], down_all[hop - 1, :, columns], preferred_element_type=jnp.float32
                )
            for mate in mates:
                disp_copy(block, chunk, mate).wait_send()
            disp_ref[block, chunk] = made.astype(jnp.bfloat16)
            for mate in mates:
                back_copy(block, chunk, mate).start()
            back_ref[block, chunk, span(member)] = disp_ref[block, chunk, span(member)]

    def weighted(block, chunk):
        one, two, meta = named(block)
        shares = jnp.where(one, meta[2:3], 0.0) + jnp.where(two, meta[3:4], 0.0)
        high = shares.astype(jnp.bfloat16)
        low = (shares - high.astype(jnp.float32)).astype(jnp.bfloat16)
        plane_arrived(back_ref, back_recv, block, chunk)
        values = back_ref[block, chunk]
        return lax.dot_general(high, values, TN, preferred_element_type=jnp.float32) + (
            lax.dot_general(low, values, TN, preferred_element_type=jnp.float32)
        )

    def start_sum(block):
        downward = block < group

        @pl.when((downward & (group == last)) | ((block > group) & (group == 0)))
        def _():
            for chunk in range(chunks):
                tok_all[block, chunk] = weighted(block, chunk).astype(jnp.bfloat16)
                sum_copy(block, chunk, downward).start()

    def relay_sent(block, chunk):
        @pl.when(block < group)
        def _():
            relay(block, chunk, True).wait_send()

        @pl.when(block > group)
        def _():
            relay(block, chunk, False).wait_send()

    def pass_sum(valid, block, chunk, downward):
        @pl.when(valid)
        def _():
            total = weighted(block, chunk)
            relay_sent(block, chunk)
            arrived(sum_in.at[block, chunk], sum_recv.at[block * chunks + chunk])
            tok_all[block, chunk] = (
                total + sum_in[block, chunk].astype(jnp.float32)
            ).astype(jnp.bfloat16)
            sum_copy(block, chunk, downward).start()

    def both(distance, action):
        @pl.when(group >= distance)
        def _():
            action(group - distance)

        @pl.when((distance > 0) & (group + distance < n_outer))
        def _():
            action(group + distance)

    lane = lax.broadcasted_iota(jnp.int32, (1, 2 * QK_ROPE), 1)
    early = lane % QK_ROPE < QK_ROPE // 2

    def rotated(values, first):
        where = pl.ds(pl.multiple_of(first, values.shape[0]), values.shape[0])
        values = values.astype(jnp.float32)
        swapped = jnp.where(
            early,
            pltpu.roll(values, 2 * QK_ROPE - QK_ROPE // 2, 1),
            pltpu.roll(values, QK_ROPE // 2, 1),
        )
        return values * table_ref[0, where] + swapped * table_ref[1, where]

    loaded(inverse_ref)
    angles = (
        sp * queries + lax.broadcasted_iota(jnp.int32, (queries, 2 * QK_ROPE), 0)
    ).astype(jnp.float32) * inverse_ref[...]
    table_ref[0] = jnp.cos(angles)
    sines = jnp.sin(angles)
    table_ref[1] = jnp.where(early, -sines, sines)
    loaded(key_rope_ref)
    turned = key_rope_ref[...].astype(jnp.float32)
    wide_rope = jnp.concatenate([turned] * 2, axis=0).T
    loaded(latent_ref)
    key_rot = rotated(wide_rope, tp * rows)
    kv_ref[sp, tp, :rows] = latent_ref[...]
    for pair in range(latent_width // (2 * QK_ROPE)):
        low = key_rot[(2 * pair) * packed : (2 * pair + 1) * packed]
        high = key_rot[(2 * pair + 1) * packed : (2 * pair + 2) * packed]
        kv_ref[sp, tp, rows:, pair * 2 * QK_ROPE : (pair + 1) * 2 * QK_ROPE] = jnp.where(
            lane < QK_ROPE, low, high
        ).astype(jnp.bfloat16)

    loaded(routes_ref, share_ref)
    experts = lax.broadcasted_iota(jnp.int32, (n_inner * n_outer, rows), 0)
    chosen = [routes_ref[slot : slot + 1] == experts for slot in range(2)]
    named_here = jnp.where(chosen[0] | chosen[1], 1.0, 0.0).astype(jnp.bfloat16)
    earlier = jnp.where(
        lax.broadcasted_iota(jnp.int32, (rows, rows), 0)
        < lax.broadcasted_iota(jnp.int32, (rows, rows), 1),
        1.0,
        0.0,
    ).astype(jnp.bfloat16)
    ranks = jnp.dot(named_here, earlier, preferred_element_type=jnp.float32)
    for slot in range(2):
        number = jnp.where(chosen[slot], ranks + (experts * cap).astype(jnp.float32), 0.0)
        meta_ref[slot : slot + 1] = jnp.sum(number, axis=0, keepdims=True)
    meta_ref[2:4] = share_ref[...]
    meta_ref[4:8] = jnp.zeros((4, rows), jnp.float32)
    meta_all[group] = meta_ref[...]

    greet(others + [at(group, mate) for mate in mates] + twins)

    for item in twin_copies(sp):
        item.start()
    for step in range(1, max(n_inner, n_outer)):
        if step < n_outer:

            @pl.when(group + step < n_outer)
            def _():
                plane_copy_kv(step).start()

        if step < n_inner:

            @pl.when(places[step] > member)
            def _():
                mate_copy(0, step).start()

    for step in range(n_outer - 1):
        meta_copy(step).start()
    loaded(rope_ref, nope_ref, value_up_ref)
    for pair in range(0, heads, 2):
        turn = rotated(rope_ref[:, pair * QK_ROPE : (pair + 2) * QK_ROPE], 0).T
        for head in (pair, pair + 1):
            columns = slice(head * QK_NOPE, (head + 1) * QK_NOPE)
            query_ref[head, :QK_NOPE] = nope_ref[:, columns].astype(jnp.float32).T.astype(
                jnp.bfloat16
            )
            query_ref[head, QK_NOPE : QK_NOPE + QK_ROPE] = turn[
                (head - pair) * QK_ROPE : (head - pair + 1) * QK_ROPE
            ].astype(jnp.bfloat16)
            query_ref[head, QK_NOPE + QK_ROPE :] = jnp.zeros(
                (QK_ROPE, queries), jnp.bfloat16
            )
    value_ref[...] = value_up_ref[...].astype(jnp.float32).T.astype(jnp.bfloat16)

    def attend(blocks, own):
        latents, rots = [], []
        for block in blocks:
            for core in range(n_tp):
                latents.append(kv_ref[block, core, :rows])
                for pair in range(latent_width // (2 * QK_ROPE)):
                    part = kv_ref[
                        block, core, rows:, pair * 2 * QK_ROPE : (pair + 1) * 2 * QK_ROPE
                    ].astype(jnp.float32)
                    rots.append(part.astype(jnp.bfloat16))
                    rots.append(pltpu.roll(part, QK_ROPE, 1).astype(jnp.bfloat16))
        latent = jnp.concatenate(latents, axis=0)
        rot = jnp.concatenate(rots, axis=0)
        count = latent.shape[0]
        keys = jnp.dot(latent, key_up_ref[...], preferred_element_type=jnp.float32).astype(
            jnp.bfloat16
        )
        values = lax.dot_general(
            value_ref[...], latent, NT, preferred_element_type=jnp.float32
        ).astype(jnp.bfloat16)
        if own:
            allowed = (
                lax.broadcasted_iota(jnp.int32, (count, queries), 0) // SEGMENT
                <= lax.broadcasted_iota(jnp.int32, (count, queries), 1) // SEGMENT
            )
        for head in range(heads):
            wide = jnp.concatenate([keys[:, head * QK_NOPE : (head + 1) * QK_NOPE], rot], axis=1)
            scores = jnp.dot(wide, query_ref[head], preferred_element_type=jnp.float32)
            if own:
                scores = jnp.where(allowed, scores, NEG_LARGE)
            new_max = jnp.max(scores, axis=0, keepdims=True)
            if not own:
                old_max = max_ref[head]
                new_max = jnp.maximum(old_max, new_max)
                shrink = jnp.exp2((old_max - new_max) * scale)
            weights = jnp.exp2((scores - new_max) * scale)
            total = jnp.sum(weights, axis=0, keepdims=True)
            product = jnp.dot(
                values[head * V_DIM : (head + 1) * V_DIM],
                weights.astype(jnp.bfloat16),
                preferred_element_type=jnp.float32,
            )
            max_ref[head] = new_max
            if own:
                sum_ref[head] = total
                acc_ref[head] = product
            else:
                sum_ref[head] = sum_ref[head] * shrink + total
                acc_ref[head] = acc_ref[head] * shrink + product

    def from_plane(distance):
        block = (group - distance) * n_inner + member
        landed(block, tp)
        for step in range(1, n_inner):
            mate_copy(distance, step).start()
        for item in twin_copies(block):
            item.start()

    def from_mate(distance, step):
        block = (group - distance) * n_inner + places[step]
        landed(block, tp)
        for item in twin_copies(block):
            item.start()

    def ready(distance, step):
        block = (group - distance) * n_inner + places[step]
        for core in cores:
            landed(block, core)
        return block

    loaded(key_up_ref)
    attend([ready(0, 0)], True)

    @pl.when(group >= 1)
    def _():
        from_plane(1)

    for step in range(1, n_inner):

        @pl.when(places[step] < member)
        def _():
            from_mate(0, step)

    for item in weight_copies():
        item.start()

    @pl.when(group >= 2)
    def _():
        from_plane(2)

    def inside(step, carry):
        mate = (member + step) % n_inner

        @pl.when(mate < member)
        def _():
            block = group * n_inner + mate
            for core in cores:
                landed(block, core)
            attend([block], False)

        return carry

    lax.fori_loop(1, n_inner, inside, 0)

    unit = 2 if n_inner % 2 == 0 else 1

    def lead(distance, first):
        for step in range(first, first + unit):
            if step > 0:
                from_mate(distance, step)

    @pl.when(group >= 1)
    def _():
        lead(1, 0)

    def outside(distance, carry):
        @pl.when(distance + 2 <= group)
        def _():
            from_plane(distance + 2)

        for first in range(0, n_inner, unit):
            if first + unit < n_inner:
                lead(distance, first + unit)
            else:

                @pl.when(distance < group)
                def _():
                    lead(distance + 1, 0)

            attend([ready(distance, step) for step in range(first, first + unit)], False)
        return carry

    lax.fori_loop(1, group + 1, outside, 0)

    def heads_copy(hop):
        return copy(
            own_ref.at[pl.ds(pl.multiple_of(cores[hop] * rows, rows), rows)],
            heads_ref.at[hop],
            heads_send.at[hop],
            heads_recv.at[hop],
            twins[hop],
        )

    for head in range(heads):
        own_ref[:, head * V_DIM : (head + 1) * V_DIM] = (
            (acc_ref[head] / sum_ref[head]).T.astype(own_ref.dtype)
        )
    for hop in range(n_tp - 1):
        heads_copy(hop).start()
    loaded(proj_ref, residual_ref, gain_ref)
    depth = heads * V_DIM

    def proj(core, columns):
        return proj_ref[pl.ds(pl.multiple_of(core * depth, depth), depth), columns]

    mine = own_ref[pl.ds(pl.multiple_of(tp * rows, rows), rows)]
    spans = [slice(chunk * width, (chunk + 1) * width) for chunk in range(chunks)]
    sums = []
    for columns in spans:
        sums.append(
            residual_ref[:, columns].astype(jnp.float32)
            + jnp.dot(mine, proj(tp, columns), preferred_element_type=jnp.float32)
        )
    for hop in range(n_tp - 1):
        arrived(heads_ref.at[hop], heads_recv.at[hop])
        for number, columns in enumerate(spans):
            sums[number] = sums[number] + jnp.dot(
                heads_ref[hop],
                proj((tp + n_tp - hop - 1) % n_tp, columns),
                preferred_element_type=jnp.float32,
            )
    square = jnp.zeros((rows, 1), jnp.float32)
    for number, columns in enumerate(spans):
        hidden = sums[number].astype(jnp.bfloat16)
        hidden_ref[:, columns] = hidden
        hidden = hidden.astype(jnp.float32)
        square = square + jnp.sum(hidden * hidden, axis=1, keepdims=True)
    factor = lax.rsqrt(square / (width * chunks) + EPSILON)
    for chunk, columns in enumerate(spans):
        tok_all[group, chunk] = (
            hidden_ref[:, columns].astype(jnp.float32) * factor * gain_ref[:, columns]
        ).astype(jnp.bfloat16)

        @pl.when(has_above)
        def _():
            relay(group, chunk, True).start()

        @pl.when(has_below)
        def _():
            relay(group, chunk, False).start()

    for chunk in range(chunks):
        scatter(group, chunk)

    def receive(block, chunk, upward):
        number = block * chunks + chunk
        arrived(tok_all.at[block, chunk], tok_recv.at[number])
        if chunk == 0:
            arrived(meta_all.at[block], meta_recv.at[block])

        @pl.when(has_above if upward else has_below)
        def _():
            relay(block, chunk, upward).start()

        scatter(block, chunk)

    def stage(distance, carry):
        for chunk in range(chunks):

            @pl.when(group >= distance)
            def _():
                receive(group - distance, chunk, True)

            @pl.when(group + distance < n_outer)
            def _():
                receive(group + distance, chunk, False)

            if chunk == EXPERT_LAG % chunks:

                @pl.when(distance == 1)
                def _():
                    loaded(gate_ref, up_ref, down_ref)
                    for item in weight_copies():
                        item.wait_recv()

                both(distance - 1, expert)
            if chunk == SUM_LAG % chunks:
                both(distance - 1, start_sum)
        return carry

    lax.fori_loop(1, n_outer, stage, 0)
    both(last, expert)
    both(last, start_sum)

    def sum_stage(distance, carry):
        low_first = 2 * group >= n_outer
        low, high = last - distance, distance + 0
        low_valid = (low < group) & has_above
        high_valid = (high > group) & has_below
        first = jnp.where(low_first, low, high)
        second = jnp.where(low_first, high, low)
        first_valid = (low_first & low_valid) | (jnp.logical_not(low_first) & high_valid)
        second_valid = (low_first & high_valid) | (jnp.logical_not(low_first) & low_valid)
        lag = chunks // 2
        for step in range(chunks + lag):
            if step < chunks:
                pass_sum(first_valid, first, step, first < group)
            if step >= lag:
                pass_sum(second_valid, second, step - lag, second < group)
        return carry

    lax.fori_loop(1, n_outer, sum_stage, 0)

    for chunk in range(chunks):
        columns = slice(chunk * width, (chunk + 1) * width)
        total = weighted(group, chunk) + hidden_ref[:, columns].astype(jnp.float32)
        sides = []
        for side, slot in ((has_above, group), (has_below, n_outer)):

            @pl.when(side)
            def _(slot=slot):
                arrived(sum_in.at[slot, chunk], sum_recv.at[slot * chunks + chunk])

            sides.append(
                jnp.where(side, sum_in[slot, chunk].astype(jnp.float32), 0.0)
            )
        out_ref[:, columns] = (total + sides[0] + sides[1]).astype(out_ref.dtype)

    for hop in range(n_tp - 1):
        heads_copy(hop).wait_send()
    for item in twin_copies(sp):
        item.wait_send()
    for step in range(1, n_outer):

        @pl.when(group + step < n_outer)
        def _():
            plane_copy_kv(step).wait_send()

    for step in range(1, n_inner):

        @pl.when(places[step] > member)
        def _():
            mate_copy(0, step).wait_send()

        @pl.when(places[step] < member)
        def _():
            for item in twin_copies(group * n_inner + places[step]):
                item.wait_send()

    def drain_kv(distance, carry):
        for step in range(n_inner):
            if step > 0:
                mate_copy(distance, step).wait_send()
            for item in twin_copies((group - distance) * n_inner + places[step]):
                item.wait_send()
        return carry

    lax.fori_loop(1, group + 1, drain_kv, 0)
    for step in range(n_outer - 1):
        meta_copy(step).wait_send()
    for item in weight_copies():
        item.wait_send()
    for chunk in range(chunks):

        @pl.when(has_above)
        def _():
            relay(group, chunk, True).wait_send()

        @pl.when(has_below)
        def _():
            relay(group, chunk, False).wait_send()

    def drain(block, carry):
        for chunk in range(chunks):
            for mate in mates:
                back_copy(block, chunk, mate).wait_send()

            @pl.when(block != group)
            def _():
                sum_copy(block, chunk, block < group).wait_send()

        return carry

    lax.fori_loop(0, n_outer, drain, 0)


EXPERT_LAG = 0
SUM_LAG = 1
NT = (((1,), (1,)), ((), ()))
TN = (((0,), (0,)), ((), ()))


def layer(inputs, n_sp, n_tp):
    (inverse, routes, share, latent, key_rope, rope, nope) = inputs[:7]
    (key_up, value_up, gain, residual, proj, gate, up, down) = inputs[7:]
    n_inner = math.gcd(n_sp, 4)
    n_outer = n_sp // n_inner
    queries = nope.shape[0]
    heads = nope.shape[1] // QK_NOPE
    rows, latent_width = latent.shape
    packed = rows // (latent_width // QK_ROPE)
    capacity = max(2, 2 * (rows * n_tp) // n_sp)
    capacity = -(-capacity // 16) * 16
    chunks = math.gcd(residual.shape[1] // 128, 4)
    part = residual.shape[1] // chunks
    slots = n_inner * capacity
    blocks = n_outer * chunks
    dma = pltpu.SemaphoreType.DMA
    vmem = pltpu.VMEM
    low, wide = jnp.bfloat16, jnp.float32
    return pl.pallas_call(
        functools.partial(layer_kernel, n_outer, n_inner, n_tp, chunks, capacity),
        out_shape=jax.ShapeDtypeStruct(residual.shape, low),
        in_specs=[pl.BlockSpec(memory_space=pltpu.HBM)] * len(inputs),
        out_specs=VMEM,
        scratch_shapes=[vmem(item.shape, item.dtype) for item in inputs]
        + [
            vmem((2, queries, 2 * QK_ROPE), wide),
            vmem((n_sp, n_tp, rows + packed, latent_width), low),
            vmem((heads, QK_NOPE + 2 * QK_ROPE, queries), low),
            vmem((heads * V_DIM, latent_width), low),
            vmem((heads, 1, queries), wide),
            vmem((heads, 1, queries), wide),
            vmem((heads, V_DIM, queries), wide),
            vmem((queries, heads * V_DIM), low),
            vmem((n_tp - 1, rows, heads * V_DIM), low),
            vmem(residual.shape, low),
            vmem((n_outer, chunks, rows, part), low),
            vmem((8, rows), wide),
            vmem((n_outer, 8, rows), wide),
            vmem((n_outer, chunks, slots, part), low),
            vmem((n_outer, chunks, slots, part), low),
            vmem((n_outer, chunks, slots, part), low),
            vmem((n_outer + 1, chunks, rows, part), low),
            vmem((n_tp - 1,) + gate.shape, low),
            vmem((n_tp - 1,) + up.shape, low),
            vmem((n_tp - 1,) + down.shape, low),
            dma((len(inputs),)),
            dma((n_outer,)),
            dma((n_sp,)),
            dma((n_sp * (n_tp - 1),)),
            dma((n_sp * n_tp,)),
            dma((n_tp - 1,)),
            dma((n_tp - 1,)),
            dma((n_outer - 1,)),
            dma((n_outer,)),
            dma((blocks,)),
            dma((blocks,)),
            dma((blocks,)),
            dma((blocks * n_inner,)),
            dma((blocks * n_inner,)),
            dma((blocks * n_inner,)),
            dma((blocks * n_inner,)),
            dma((blocks,)),
            dma((blocks + chunks,)),
            dma((3 * (n_tp - 1),)),
            dma((3 * (n_tp - 1),)),
        ],
        compiler_params=pltpu.CompilerParams(
            collective_id=0, has_side_effects=True, vmem_limit_bytes=VMEM_LIMIT
        ),
        name="layer",
    )(*inputs)


VMEM_LIMIT = 60 * 2**20


def local(
    residual,
    query_nope,
    query_rope,
    latent,
    key_rope,
    key_up,
    value_up,
    out_proj,
    norm_gain,
    routes,
    route_weight,
    w_gate,
    w_up,
    w_down,
):
    half = QK_ROPE // 2
    inverse = np.tile(ROPE_BASE ** (-2.0 * np.arange(half) / QK_ROPE), 4).astype(np.float32)
    return layer(
        [
            jnp.asarray(inverse[None, :]),
            routes.T,
            route_weight.T,
            latent,
            key_rope.T,
            query_rope,
            query_nope,
            key_up,
            value_up,
            norm_gain[None, :],
            residual,
            out_proj,
            w_gate[0],
            w_up[0],
            w_down[0],
        ],
        lax.axis_size("sp"),
        lax.axis_size("tp"),
    )


def solution(mesh):
    return jax.shard_map(
        local,
        mesh=mesh,
        in_specs=(
            P(("sp", "tp"), None),
            P("sp", "tp"),
            P("sp", "tp"),
            P(("sp", "tp"), None),
            P(("sp", "tp"), None),
            P(None, "tp"),
            P(None, "tp"),
            P(),
            P(),
            P(("sp", "tp"), None),
            P(("sp", "tp"), None),
            P("sp", None, "tp"),
            P("sp", None, "tp"),
            P("sp", "tp", None),
        ),
        out_specs=P(("sp", "tp"), None),
        check_vma=False,
    )
```

time: 152 us -> 111 us (0.73)
  Pallas kernels: 134 us -> 109 us
  local copies, waits for them, and re-layouts: 7.47 us -> 1.88 us
  other arithmetic: 5.47 us -> 0 us
  matrix products: 4.44 us -> 0 us
    pallas_call x4 -> x1, Pallas kernels: 134 us -> 109 us  [layer(): pl.pallas_call(functools.partial(layer_kernel, n_outer, n_inner, n_tp, ch...]
    dot_general x2 -> x0, matrix products: 4.44 us -> none  [the longest x1 2.32 us: local(): jnp.dot(all_heads[core], proj_parts[core], preferred_element_type=jnp.flo...]
    unnamed x17 -> x1, local copies, waits for them, and re-layouts: 5.55 us -> 1.88 us
    concatenate x2 -> x0, other arithmetic: 2.22 us -> none  [the longest x1 1.55 us: local(): jnp.concatenate([latent, key_rot, jnp.zeros((row_count, width_pad), jnp.b...]
where the time goes in v3:
time: 111 us
  Pallas kernels  109 us (98%)
  local copies, waits for them, and re-layouts  1.88 us (2%)
    pallas_call x1, Pallas kernels, layer(): pl.pallas_call(functools.partial(layer_kernel, n_outer, n_inner, n_tp, ch...  109 us

profile of v3, /device:TPU:0, one launch (start us, length us, event | category | flops | bytes accessed | tf_op | source)
XLA Modules:
  0.0 111.3 jit_solution(15764984228541763108)
XLA Ops:
  0.0 109.4 %layer.1 = bf16[128,2048]{1,0:T(8,128)(2,1)} custom-call(f32[1,128]{1,0:T(1,128)} %constant.2.clone.inverse_hbm, s32[2,128]{1,0:T(2,128)} %bitcast.12, f32[2,128]{1,0:T(2,128)} %bitcast.13, bf16[128,256]{1,0:T(8,128)(2,1)} %latent_hbm.1, bf16[64,128]{1,0:T(8,128)(2,1)} %bitcast.10, bf16[256,256]{1,0:T(8,128)(2,1)} %rope_hbm.1, bf16[256,512]{1,0:T(8,128)(2,1)} %nope_hbm.1, ...), custom_call_target="tpu_custom_call" | custom-call | tf_op jit(solution)/shard_map/layer/pallas_call | solution.py:785
  109.4 1.9 %copy.17 = bf16[128,2048]{1,0:T(8,128)(2,1)} copy(bf16[128,2048]{1,0:T(8,128)(2,1)} %layer.1) | data formatting | bytes 1048576

commit v4 on v3

--- a/solution.py
+++ b/solution.py
@@ -103,6 +103,7 @@
     meta_recv,
     above_send,
     below_send,
+    far_send,
     tok_recv,
     disp_send,
     disp_recv,
@@ -209,6 +210,20 @@
         peer = at(group + 1 if upward else group - 1, member)
         return copy(ref, ref, sems.at[number], tok_recv.at[number], peer)
 
+    sends_far = (group == 0) & (n_outer > 2)
+
+    def passes(block):
+        return has_above & ((n_outer == 2) | (block != 0) | (group != last - 1))
+
+    def far_copy(chunk):
+        ref = tok_all.at[group, chunk]
+        number = group * chunks + chunk
+        return copy(ref, ref, far_send.at[chunk], tok_recv.at[number], at(last, member))
+
+    def below(order):
+        first_far = (group == last) & (n_outer > 2)
+        return group - jnp.where(first_far, jnp.where(order == 1, last, order - 1), order)
+
     def plane_copy(source, target, send_sem, recv_sem, block, chunk, mate):
         number = (block * chunks + chunk) * n_inner
         return copy(
@@ -318,7 +333,7 @@
                 sum_copy(block, chunk, downward).start()
 
     def relay_sent(block, chunk):
-        @pl.when(block < group)
+        @pl.when((block < group) & passes(block))
         def _():
             relay(block, chunk, True).wait_send()
 
@@ -340,7 +355,7 @@
     def both(distance, action):
         @pl.when(group >= distance)
         def _():
-            action(group - distance)
+            action(jnp.where(distance == 0, group, below(distance)))
 
         @pl.when((distance > 0) & (group + distance < n_outer))
         def _():
@@ -515,15 +530,23 @@
         def _():
             from_mate(0, step)
 
-    for item in weight_copies():
-        item.start()
-
     @pl.when(group >= 2)
     def _():
         from_plane(2)
 
+    unit = 2 if n_inner % 2 == 0 else 1
+
+    def lead(distance, first):
+        for step in range(first, first + unit):
+            if step > 0:
+                from_mate(distance, step)
+
     def inside(step, carry):
         mate = (member + step) % n_inner
+
+        @pl.when((step == n_inner - 1) & (group >= 1))
+        def _():
+            lead(1, 0)
 
         @pl.when(mate < member)
         def _():
@@ -535,17 +558,6 @@
         return carry
 
     lax.fori_loop(1, n_inner, inside, 0)
-
-    unit = 2 if n_inner % 2 == 0 else 1
-
-    def lead(distance, first):
-        for step in range(first, first + unit):
-            if step > 0:
-                from_mate(distance, step)
-
-    @pl.when(group >= 1)
-    def _():
-        lead(1, 0)
 
     def outside(distance, carry):
         @pl.when(distance + 2 <= group)
@@ -581,6 +593,8 @@
         )
     for hop in range(n_tp - 1):
         heads_copy(hop).start()
+    for item in weight_copies():
+        item.start()
     loaded(proj_ref, residual_ref, gain_ref)
     depth = heads * V_DIM
 
@@ -623,6 +637,11 @@
         def _():
             relay(group, chunk, False).start()
 
+    @pl.when(sends_far)
+    def _():
+        for chunk in range(chunks):
+            far_copy(chunk).start()
+
     for chunk in range(chunks):
         scatter(group, chunk)
 
@@ -632,7 +651,7 @@
         if chunk == 0:
             arrived(meta_all.at[block], meta_recv.at[block])
 
-        @pl.when(has_above if upward else has_below)
+        @pl.when(passes(block) if upward else has_below)
         def _():
             relay(block, chunk, upward).start()
 
@@ -643,23 +662,28 @@
 
             @pl.when(group >= distance)
             def _():
-                receive(group - distance, chunk, True)
+                receive(below(distance), chunk, True)
 
             @pl.when(group + distance < n_outer)
             def _():
                 receive(group + distance, chunk, False)
 
-            if chunk == EXPERT_LAG % chunks:
-
-                @pl.when(distance == 1)
+            if chunk in (EXPERT_EARLY, chunks - 1):
+
+                @pl.when(((group > 0) & (group < last)) == (chunk == chunks - 1))
                 def _():
-                    loaded(gate_ref, up_ref, down_ref)
-                    for item in weight_copies():
-                        item.wait_recv()
-
-                both(distance - 1, expert)
-            if chunk == SUM_LAG % chunks:
-                both(distance - 1, start_sum)
+                    @pl.when(distance == 1)
+                    def _():
+                        loaded(gate_ref, up_ref, down_ref)
+                        for item in weight_copies():
+                            item.wait_recv()
+
+                    both(distance - 1, expert)
+
+        @pl.when(distance > 1)
+        def _():
+            both(distance - 1, start_sum)
+
         return carry
 
     lax.fori_loop(1, n_outer, stage, 0)
@@ -667,23 +691,18 @@
     both(last, start_sum)
 
     def sum_stage(distance, carry):
-        low_first = 2 * group >= n_outer
-        low, high = last - distance, distance + 0
-        low_valid = (low < group) & has_above
+        low, high = distance - (last - group), distance + 1
+        low_valid = (low >= 0) & (low < group) & has_above
         high_valid = (high > group) & has_below
-        first = jnp.where(low_first, low, high)
-        second = jnp.where(low_first, high, low)
-        first_valid = (low_first & low_valid) | (jnp.logical_not(low_first) & high_valid)
-        second_valid = (low_first & high_valid) | (jnp.logical_not(low_first) & low_valid)
-        lag = chunks // 2
+        lag = SUM_GAP
         for step in range(chunks + lag):
             if step < chunks:
-                pass_sum(first_valid, first, step, first < group)
+                pass_sum(high_valid, high, step, False)
             if step >= lag:
-                pass_sum(second_valid, second, step - lag, second < group)
+                pass_sum(low_valid, low, step - lag, True)
         return carry
 
-    lax.fori_loop(1, n_outer, sum_stage, 0)
+    lax.fori_loop(1, last, sum_stage, 0)
 
     for chunk in range(chunks):
         columns = slice(chunk * width, (chunk + 1) * width)
@@ -736,6 +755,10 @@
         item.wait_send()
     for chunk in range(chunks):
 
+        @pl.when(sends_far)
+        def _():
+            far_copy(chunk).wait_send()
+
         @pl.when(has_above)
         def _():
             relay(group, chunk, True).wait_send()
@@ -758,8 +781,8 @@
     lax.fori_loop(0, n_outer, drain, 0)
 
 
-EXPERT_LAG = 0
-SUM_LAG = 1
+SUM_GAP = 0
+EXPERT_EARLY = 1
 NT = (((1,), (1,)), ((), ()))
 TN = (((0,), (0,)), ((), ()))
 
@@ -820,6 +843,7 @@
             dma((n_outer,)),
             dma((blocks,)),
             dma((blocks,)),
+            dma((chunks,)),
             dma((blocks,)),
             dma((blocks * n_inner,)),
             dma((blocks * n_inner,)),

time: 111 us -> 106 us (0.955)
  the two profiles are of different devices: /device:TPU:0 before, /device:TPU:8 now
where the time goes in v4:
time: 106 us
  Pallas kernels  104 us (98%)
  local copies, waits for them, and re-layouts  1.88 us (2%)
    pallas_call x1, Pallas kernels, layer(): pl.pallas_call(functools.partial(layer_kernel, n_outer, n_inner, n_tp, ch...  104 us

profile of v4, /device:TPU:8, one launch (start us, length us, event | category | flops | bytes accessed | tf_op | source)
XLA Modules:
  0.0 106.0 jit_solution(17051444687119302170)
XLA Ops:
  0.0 104.2 %layer.1 = bf16[128,2048]{1,0:T(8,128)(2,1)} custom-call(f32[1,128]{1,0:T(1,128)} %constant.2.clone.inverse_hbm, s32[2,128]{1,0:T(2,128)} %bitcast.12, f32[2,128]{1,0:T(2,128)} %bitcast.13, bf16[128,256]{1,0:T(8,128)(2,1)} %latent_hbm.1, bf16[64,128]{1,0:T(8,128)(2,1)} %bitcast.10, bf16[256,256]{1,0:T(8,128)(2,1)} %rope_hbm.1, bf16[256,512]{1,0:T(8,128)(2,1)} %nope_hbm.1, ...), custom_call_target="tpu_custom_call" | custom-call | tf_op jit(solution)/shard_map/layer/pallas_call | solution.py:808
  104.2 1.9 %copy.17 = bf16[128,2048]{1,0:T(8,128)(2,1)} copy(bf16[128,2048]{1,0:T(8,128)(2,1)} %layer.1) | data formatting | bytes 1048576

commit v5 on v4

--- a/solution.py
+++ b/solution.py
@@ -500,10 +500,10 @@
     def from_plane(distance):
         block = (group - distance) * n_inner + member
         landed(block, tp)
-        for step in range(1, n_inner):
-            mate_copy(distance, step).start()
         for item in twin_copies(block):
             item.start()
+        for step in range(n_inner - 1, 0, -1):
+            mate_copy(distance, step).start()
 
     def from_mate(distance, step):
         block = (group - distance) * n_inner + places[step]

time: 106 us -> 106 us (level)
  no operation moved by 1% of the time
where the time goes in v5:
time: 106 us
  Pallas kernels  104 us (98%)
  local copies, waits for them, and re-layouts  1.88 us (2%)
    pallas_call x1, Pallas kernels, layer(): pl.pallas_call(functools.partial(layer_kernel, n_outer, n_inner, n_tp, ch...  104 us

profile of v5, /device:TPU:8, one launch (start us, length us, event | category | flops | bytes accessed | tf_op | source)
XLA Modules:
  0.0 105.9 jit_solution(5245512355623605418)
XLA Ops:
  0.0 104.0 %layer.1 = bf16[128,2048]{1,0:T(8,128)(2,1)} custom-call(f32[1,128]{1,0:T(1,128)} %constant.2.clone.inverse_hbm, s32[2,128]{1,0:T(2,128)} %bitcast.12, f32[2,128]{1,0:T(2,128)} %bitcast.13, bf16[128,256]{1,0:T(8,128)(2,1)} %latent_hbm.1, bf16[64,128]{1,0:T(8,128)(2,1)} %bitcast.10, bf16[256,256]{1,0:T(8,128)(2,1)} %rope_hbm.1, bf16[256,512]{1,0:T(8,128)(2,1)} %nope_hbm.1, ...), custom_call_target="tpu_custom_call" | custom-call | tf_op jit(solution)/shard_map/layer/pallas_call | solution.py:808
  104.0 1.9 %copy.17 = bf16[128,2048]{1,0:T(8,128)(2,1)} copy(bf16[128,2048]{1,0:T(8,128)(2,1)} %layer.1) | data formatting | bytes 1048576
